TPU v7x, 128 devices: a whole 4x4x4 slice. The times are simulated.
128 devices in a mesh: sp: 16 (over z, x), tp: 8 (over y, core).
Axes of the slice: x: 4, y: 4, z: 4, core: 2. Of those that a mesh axis runs over, the one named last changes fastest.
Arguments:
- tokens: bfloat16 [12288, 2048], P('sp', 'tp'), may hold values from -23 to 23, as said below
- norm_gain: float32 [2048], replicated, may hold values from 0.8 to 8, as said below
- window_query: bfloat16 [2048, 1024], P(None, 'tp'), may hold values from -0.125 to 0.125
- window_key: bfloat16 [2048, 512], P(None, 'tp'), may hold values from -0.125 to 0.125
- window_value: bfloat16 [2048, 512], P(None, 'tp'), may hold values from -0.125 to 0.125
- sink_logit: float32 [16], P('tp'), may hold values from 2 to 6
- down_query: bfloat16 [2048, 768], replicated, may hold values from -0.125 to 0.125
- down_latent: bfloat16 [2048, 512], replicated, may hold values from -0.125 to 0.125
- rotary_proj: bfloat16 [2048, 32], replicated, may hold values from -0.125 to 0.125
- query_gain: float32 [768], replicated, may hold values from 0.8 to 8, as said below
- latent_gain: float32 [512], replicated, may hold values from 0.8 to 8, as said below
- up_query: bfloat16 [768, 1536], P(None, 'tp'), may hold values from -0.21875 to 0.21875
- up_key: bfloat16 [512, 1024], P(None, 'tp'), may hold values from -0.25 to 0.25
- up_value: bfloat16 [512, 1024], P(None, 'tp'), may hold values from -0.25 to 0.25
- window_out: bfloat16 [1024, 2048], P('tp'), may hold values from -0.125 to 0.125
- latent_out: bfloat16 [1024, 2048], P('tp'), may hold values from -0.125 to 0.125
Outputs:
- mixed: bfloat16 [12288, 2048], P(('sp', 'tp'))
Inputs may be any that keep to these rules, and one draw needn't show every extreme that they name: `tokens`: real-valued; the channels carry scales that vary smoothly by a factor of up to twenty across the width. `norm_gain`: positive. `query_gain`: positive. `latent_gain`: positive.
All inputs are finite; a program needn't handle non-finite values.
Results may differ from a plain program's by a relative error of at most 0.04.
The roundings to bfloat16 on the way count: a program that leaves them out, or rounds other values in their place, can miss the bound.
Values may be sent and summed in bfloat16 or wider, within the bound.
A program may use at most 128 MiB of HBM per device.

v0:
```python
import jax
import jax.numpy as jnp
from jax import lax
from jax.sharding import PartitionSpec as P

D = 2048
A_HEADS = 16
HD = 64
NOPE = 64
ROPE = 32
VD = 64
WINDOW = 128
QBLOCK = 256


EPS = 1e-06
THETA = 10000.0
key_span = 1024


def with_halo(x, sides, width):
    for axis, dim in sides:
        size, length = (lax.axis_size(axis), x.shape[dim])
        up = [(i, (i + 1) % size) for i in range(size - 1)]
        down = [(j, i) for i, j in up]
        last = lax.slice_in_dim(x, length - width, length, axis=dim)
        initial = lax.slice_in_dim(x, 0, width, axis=dim)
        before = lax.ppermute(last, axis, up)
        after = lax.ppermute(initial, axis, down)
        x = jnp.concatenate([before, x, after], axis=dim)
    return x


def side_by_side(arrays, axis, dim, along):
    both = jnp.concatenate(arrays, axis=along)
    whole, at, gathered = (lax.all_gather(both, axis, axis=dim, tiled=True), 0, [])
    for a in arrays:
        gathered.append(lax.slice_in_dim(whole, at, at + a.shape[along], axis=along))
        at += a.shape[along]
    return tuple(gathered)


def rotate(vector, positions):
    half_len = vector.shape[-1] // 2
    inverse = THETA ** (-jnp.arange(half_len, dtype=jnp.float32) / half_len)
    angles = positions.astype(jnp.float32)[:, None] * inverse[None, :]
    new_shape = (angles.shape[0],) + (1,) * (vector.ndim - 2) + (half_len,)
    cosine = jnp.cos(angles).reshape(new_shape)
    sine_part = jnp.sin(angles).reshape(new_shape)
    front_half = vector[..., :half_len].astype(jnp.float32)
    second = vector[..., half_len:].astype(jnp.float32)
    return jnp.concatenate(
        [front_half * cosine - second * sine_part, second * cosine + front_half * sine_part],
        axis=-1,
    )


def norm_rows(values, gain_vec):
    as_float = values.astype(jnp.float32)
    return (
        as_float * lax.rsqrt(jnp.mean(as_float * as_float, axis=1, keepdims=True) + EPS) * gain_vec
    ).astype(jnp.bfloat16)


def attend(running, q_nope, q_rot, key_rows, value_rows, rot_keys, lat_scale):
    prior_max, denom_sum, weighted = running
    scores = (
        jnp.einsum("qhd,khd->hqk", q_nope, key_rows, preferred_element_type=jnp.float32)
        + jnp.einsum("qhr,kr->hqk", q_rot, rot_keys, preferred_element_type=jnp.float32)
    ) * lat_scale
    row_max = jnp.maximum(prior_max, jnp.max(scores, axis=2))
    rescale = jnp.exp(prior_max - row_max)
    weights = jnp.exp(scores - row_max[:, :, None])
    denom_sum = denom_sum * rescale + jnp.sum(weights, axis=2)
    weighted = weighted * rescale.T[:, :, None] + jnp.einsum(
        "hqk,khd->qhd", weights.astype(jnp.bfloat16), value_rows, preferred_element_type=jnp.float32
    )
    return (row_max, denom_sum, weighted)


def in_blocks(running, arrays, block_fn):
    key_count = arrays[0].shape[0]
    blocked = tuple(
        (member.reshape((key_count // key_span, key_span) + member.shape[1:]) for member in arrays)
    )

    def scan_step(state_now, key_block):
        return (block_fn(state_now, key_block), None)

    running, unused = lax.scan(scan_step, running, blocked)
    return running


def per_device(
    tokens,
    norm_gain,
    window_query,
    window_key,
    window_value,
    sink_logit,
    down_query,
    down_latent,
    rotary_proj,
    query_gain,
    latent_gain,
    up_query,
    up_key,
    up_value,
    window_out,
    latent_out,
):
    row_count = tokens.shape[0]
    projections = (window_query, window_key, window_value, down_query, down_latent, rotary_proj)
    start_carry = (jnp.zeros((row_count,), jnp.float32),) + tuple(
        (jnp.zeros((row_count, weight.shape[1]), jnp.float32) for weight in projections)
    )
    as_float = lax.all_gather(tokens, "tp", axis=1, tiled=True).astype(jnp.float32)
    scaled = (as_float * norm_gain[None, :]).astype(jnp.bfloat16)
    updated = [jnp.sum(as_float * as_float, axis=1)]
    for total_now, weight in zip(start_carry[1:], projections):
        updated.append(jnp.dot(scaled, weight, preferred_element_type=jnp.float32))
    folded = tuple(updated)
    row_scale = lax.rsqrt(folded[0] / D + EPS)[:, None]
    q_window, k_window, v_window, latent_q, latent_kv, rotary_rows = [
        (member * row_scale).astype(jnp.bfloat16) for member in folded[1:]
    ]
    seq_index = lax.axis_index("sp")
    positions = seq_index * row_count + jnp.arange(row_count, dtype=jnp.int32)
    heads_dev = window_query.shape[1] // HD
    kv_dev = window_key.shape[1] // HD
    group = heads_dev // kv_dev
    stacked = jnp.concatenate([k_window, v_window], axis=1)
    padded = with_halo(stacked, (("sp", 0),), WINDOW)
    span_len = QBLOCK + 2 * WINDOW
    block_count = row_count // QBLOCK
    spans = jnp.stack(
        [
            padded[block_num * QBLOCK : block_num * QBLOCK + span_len]
            for block_num in range(block_count)
        ]
    )
    key_part = spans[..., : kv_dev * HD].reshape(block_count, span_len, kv_dev, HD)
    value_part = spans[..., kv_dev * HD :].reshape(block_count, span_len, kv_dev, HD)
    queries = q_window.reshape(block_count, QBLOCK, kv_dev, group, HD)
    scores = jnp.einsum(
        "nqhgd,nkhd->nhgqk", queries, key_part, preferred_element_type=jnp.float32
    ) * HD ** (-0.5)
    distance = jnp.arange(QBLOCK)[:, None] + WINDOW - jnp.arange(span_len)[None, :]
    head_ids = lax.axis_index("tp") * heads_dev + jnp.arange(heads_dev, dtype=jnp.int32)
    slopes = jnp.exp2(-8.0 * (head_ids.astype(jnp.float32) + 1.0) / A_HEADS).reshape(kv_dev, group)
    scores = scores - slopes[None, :, :, None, None] * jnp.abs(distance).astype(jnp.float32)
    key_pos = (
        seq_index * row_count
        + (jnp.arange(block_count, dtype=jnp.int32) * QBLOCK)[:, None]
        + jnp.arange(span_len, dtype=jnp.int32)[None, :]
        - WINDOW
    )
    seq_len = row_count * lax.axis_size("sp")
    valid = (jnp.abs(distance) <= WINDOW)[None] & ((key_pos >= 0) & (key_pos < seq_len))[:, None, :]
    scores = jnp.where(valid[:, None, None], scores, -jnp.inf)
    sinks = sink_logit.reshape(kv_dev, group)[None, :, :, None, None]
    row_max = jnp.maximum(jnp.max(scores, axis=4, keepdims=True), sinks)
    weights = jnp.exp(scores - row_max)
    weights = weights / (jnp.sum(weights, axis=4, keepdims=True) + jnp.exp(sinks - row_max))
    out_window = (
        jnp.einsum(
            "nhgqk,nkhd->nqhgd",
            weights.astype(jnp.bfloat16),
            value_part,
            preferred_element_type=jnp.float32,
        )
        .astype(jnp.bfloat16)
        .reshape(row_count, heads_dev * HD)
    )
    latent_heads = up_query.shape[1] // (NOPE + ROPE)
    q_latent = jnp.dot(
        norm_rows(latent_q, query_gain), up_query, preferred_element_type=jnp.float32
    ).astype(jnp.bfloat16)
    q_latent = q_latent.reshape(row_count, latent_heads, NOPE + ROPE)
    q_nope = q_latent[..., :NOPE]
    q_rot = rotate(q_latent[..., NOPE:], positions).astype(jnp.bfloat16)
    k_rot = rotate(rotary_rows, positions).astype(jnp.bfloat16)
    normed_kv = norm_rows(latent_kv, latent_gain)
    lat_scale = (NOPE + ROPE) ** (-0.5)
    start_state = (
        jnp.full((latent_heads, row_count), -1e30, jnp.float32),
        jnp.zeros((latent_heads, row_count), jnp.float32),
        jnp.zeros((row_count, latent_heads, VD), jnp.float32),
    )
    key_rows = jnp.dot(normed_kv, up_key, preferred_element_type=jnp.float32).astype(jnp.bfloat16)
    value_rows = jnp.dot(normed_kv, up_value, preferred_element_type=jnp.float32).astype(
        jnp.bfloat16
    )
    paired = jnp.concatenate([key_rows, value_rows], axis=1)

    def split_block(running, key_block):
        pair_part, rot_part = key_block
        key_count = pair_part.shape[0]
        return attend(
            running,
            q_nope,
            q_rot,
            pair_part[:, : latent_heads * NOPE].reshape(key_count, latent_heads, NOPE),
            pair_part[:, latent_heads * NOPE :].reshape(key_count, latent_heads, VD),
            rot_part,
            lat_scale,
        )

    final_state = in_blocks(start_state, side_by_side((paired, k_rot), "sp", 0, 1), split_block)
    out_latent = (
        (final_state[2] / final_state[1].T[:, :, None])
        .astype(jnp.bfloat16)
        .reshape(row_count, latent_heads * VD)
    )
    return lax.psum_scatter(
        (
            jnp.dot(out_window, window_out, preferred_element_type=jnp.float32)
            + jnp.dot(out_latent, latent_out, preferred_element_type=jnp.float32)
        ).astype(jnp.bfloat16),
        "tp",
        scatter_dimension=0,
        tiled=True,
    )


def solution(mesh):
    placed = (
        P("sp", "tp"),
        P(),
        P(None, "tp"),
        P(None, "tp"),
        P(None, "tp"),
        P("tp"),
        P(),
        P(),
        P(),
        P(),
        P(),
        P(None, "tp"),
        P(None, "tp"),
        P(None, "tp"),
        P("tp", None),
        P("tp", None),
    )
    return jax.shard_map(
        per_device, mesh=mesh, in_specs=placed, out_specs=P(("sp", "tp"), None), check_vma=False
    )
```

profile of v0, /device:TPU:1, one launch (start us, length us, event | category | flops | bytes accessed | tf_op | source)
XLA Modules:
  0.0 245.8 jit_solution(5702129574684875817)
XLA Ops:
  7.3 36.4 %all-gather.3.cloned.1.call-done = bf16[768,2048]{1,0:T(8,128)(2,1)} async-done(((bf16[768,256]{1,0:T(8,128)(2,1)}), bf16[768,2048]{1,0:T(8,128)(2,1)}) %all-gather.3.cloned.1.call-update) | async-done | bytes 3145744 | tf_op jit(solution)/shard_map/all_gather | solution.py:117
  43.8 2.7 %fusion.19 = f32[768]{0:T(1024)S(1)} fusion(bf16[768,2048]{1,0:T(8,128)(2,1)} %all-gather.3.cloned.1.call-done), kind=kLoop, calls=%fused_computation.23 | loop fusion | flops 4717824 | bytes 3148800 | tf_op jit(solution)/shard_map/reduce_sum | solution.py:119
  46.6 3.5 %fusion.26 = (f32[768]{0:T(1024)S(1)}, bf16[768,512]{0,1:T(8,128)(2,1)S(1)}) fusion(f32[768]{0:T(1024)S(1)} %add_rsqrt_fusion.2, bf16[2048,512]{1,0:T(8,128)(2,1)} %param.25, bf16[768,2048]{1,0:T(8,128)(2,1)S(1)} %copy-done.6, f32[2048]{0:T(1024)S(1)} %copy-done.24), kind=kOutput, calls=%fused_computation.39 | convolution fusion | flops 1617296640 | bytes 6043648 | tf_op jit(solution)/shard_map/dot_general | solution.py:121
  56.4 3.1 %fusion.62 = bf16[768,64]{0,1:T(8,128)(2,1)S(1)} fusion(bf16[2048,64]{0,1:T(8,128)(2,1)} %param.22, bf16[768,2048]{1,0:T(8,128)(2,1)} %all-gather.3.cloned.1.call-done, f32[2048]{0:T(1024)} %param.19, f32[768]{0:T(1024)} %copy-done.15), kind=kOutput, calls=%fused_computation.60 | convolution fusion | flops 206143488 | bytes 3517440 | tf_op jit(solution)/shard_map/dot_general | solution.py:121
  61.4 3.7 %collective-permute-start = (bf16[128,128]{0,1:T(8,128)(2,1)}, bf16[128,128]{0,1:T(8,128)(2,1)}, u32[]{:S(2)}, u32[]{:S(2)}) collective-permute-start(bf16[128,128]{0,1:T(8,128)(2,1)} %get-tuple-element.120), channel_id=1, source_target_pairs={{0,8},{8,16},{16,24},{24,32},{32,40},{40,48},{48,56},{56,64},{64,7... | collective-permute-start | bytes 98312 | tf_op jit(solution)/shard_map/ppermute | solution.py:28
  65.1 1.6 collective-permute-start.1
  66.7 2.8 %fusion.22 = (f32[768]{0:T(1024)S(1)}, bf16[768,768]{0,1:T(8,128)(2,1)S(1)}) fusion(f32[768]{0:T(1024)S(1)} %copy-done.16, bf16[2048,768]{1,0:T(8,128)(2,1)S(1)} %copy-done, bf16[768,2048]{1,0:T(8,128)(2,1)S(1)} %copy-done.7, f32[2048]{0:T(1024)S(1)} %copy-done.25), kind=kOutput, calls=%fused_computation.32 | convolution fusion | flops 2423586048 | bytes 7485440 | tf_op jit(solution)/shard_map/dot_general | solution.py:121
  74.4 2.4 fusion.25
  79.2 3.7 %fusion.101 = f32[768,2048]{1,0:T(8,128)} fusion(bf16[768,128]{0,1:T(8,128)(2,1)S(1)} %bitcast.125, bf16[128,2048]{1,0:T(8,128)(2,1)S(1)} %copy-done.8), kind=kOutput, calls=%fused_computation.127 | convolution fusion | flops 402653184 | bytes 7012352 | tf_op jit(solution)/shard_map/dot_general | solution.py:217
  82.9 36.3 %all-gather.5.cloned.1.call-done = bf16[12288,288]{0,1:T(8,128)(2,1)} async-done(((bf16[768,288]{0,1:T(8,128)(2,1)}), bf16[12288,288]{0,1:T(8,128)(2,1)}) %all-gather.5.cloned.1.call-update) | async-done | bytes 7077904 | tf_op jit(solution)/shard_map/all_gather | solution.py:36
  119.2 6.1 %slice.77 = bf16[12288,256]{0,1:T(8,128)(2,1)} slice(bf16[12288,288]{0,1:T(8,128)(2,1)} %all-gather.5.cloned.1.call-done), slice={[0:12288], [0:256]} | slice | bytes 12582912 | tf_op jit(solution)/shard_map/slice | solution.py:38
  125.3 8.7 %copy.27 = bf16[12288,256]{1,0:T(8,128)(2,1)} copy(bf16[12288,256]{0,1:T(8,128)(2,1)} %slice.77) | data formatting | bytes 12582912 | tf_op jit(solution)/shard_map/slice | solution.py:38
  135.0 65.5 %while.15 = (s32[]{:T(128)}, f32[2,768]{1,0:T(2,128)S(1)}, f32[2,768]{1,0:T(2,128)S(1)}, f32[768,2,64]{0,2,1:T(8,128)S(1)}, bf16[12,1024,256]{2,1,0:T(8,128)(2,1...) while((s32[]{:T(128)}, f32[2,768]{1,0:T(2,128)S(1)}, ...), condition=%wide.region_8.9_spmd.clone, body=%wide.region_5.8_spmd.clone.sunk | while | flops 514630656 | bytes 36372604 | solution.py:90
  139.3 1.1 fusion.142
  144.7 1.1 fusion.142
  150.2 1.1 fusion.142
  155.7 1.1 fusion.142
  161.1 1.1 fusion.142
  172.0 1.1 fusion.142
  188.4 1.1 fusion.142
  193.9 1.1 fusion.142
  199.4 1.1 fusion.142
  200.6 5.7 %add_convert_fusion = bf16[768,2048]{1,0:T(8,128)(2,1)} fusion(f32[768,2048]{1,0:T(8,128)} %fusion.101, bf16[768,128]{0,1:T(8,128)(2,1)S(1)} %bitcast.127, bf16[128,2048]{1,0:T(8,128)(2,1)} %param.33), kind=kOutput, calls=%fused_computation.24 | convolution fusion | flops 405798912 | bytes 10158080 | tf_op jit(solution)/shard_map/dot_general | solution.py:218
  206.4 32.9 %reduce-scatter.2.cloned.1.call-done = bf16[96,2048]{1,0:T(8,128)(2,1)} async-done(((bf16[768,2048]{1,0:T(8,128)(2,1)}), bf16[96,2048]{1,0:T(8,128)(2,1)}) %reduce-scatter.2.cloned.1.call-update) | async-done | bytes 393232 | tf_op jit(solution)/shard_map/reduce_scatter | solution.py:215
  (216 shorter events, 71.3 us)
Async XLA Ops:
  6.5 60.2 %copy-start = (bf16[2048,768]{1,0:T(8,128)(2,1)S(1)}, bf16[2048,768]{1,0:T(8,128)(2,1)}, u32[]{:S(2)}) copy-start(bf16[2048,768]{1,0:T(8,128)(2,1)} %param.24) | copy-start | bytes 9437188
  6.5 40.0 %copy-start.24 = (f32[2048]{0:T(1024)S(1)}, f32[2048]{0:T(1024)}, u32[]{:S(2)}) copy-start(f32[2048]{0:T(1024)} %param.19) | copy-start | bytes 24580
  6.5 37.2 %all-gather.3.cloned.1.call-start = ((), (), s32[]{:S(2)}) async-start(), calls=%async_computation.1 | async-start | bytes 3538944 | tf_op jit(solution)/shard_map/all_gather | solution.py:117
  7.3 111.9 %all-gather.5.cloned.1.call-start = ((), (), s32[]{:S(2)}) async-start(), calls=%async_computation.2 | async-start | bytes 7520256 | tf_op jit(solution)/shard_map/all_gather | solution.py:36
  46.6 4.4 %copy-start.15 = (f32[768]{0:T(1024)}, f32[768]{0:T(1024)S(1)}, u32[]{:S(2)}) copy-start(f32[768]{0:T(1024)S(1)} %add_rsqrt_fusion.2) | copy-start | bytes 9220
  46.6 3.6 %copy-start.21 = (bf16[512,128]{1,0:T(8,128)(2,1)S(1)}, bf16[512,128]{1,0:T(8,128)(2,1)}, u32[]{:S(2)}) copy-start(bf16[512,128]{1,0:T(8,128)(2,1)} %param.31) | copy-start | bytes 393220
  46.6 3.6 %copy-start.27 = (f32[512]{0:T(512)S(1)}, f32[512]{0:T(512)}, u32[]{:S(2)}) copy-start(f32[512]{0:T(512)} %param.28) | copy-start | bytes 6148
  46.6 4.0 %copy-start.22 = (bf16[512,128]{1,0:T(8,128)(2,1)S(1)}, bf16[512,128]{1,0:T(8,128)(2,1)}, u32[]{:S(2)}) copy-start(bf16[512,128]{1,0:T(8,128)(2,1)} %param.30) | copy-start | bytes 393220
  53.8 185.4 %reduce-scatter.2.cloned.1.call-start = ((), (), s32[]{:S(2)}) async-start(), calls=%async_computation.3 | async-start | bytes 3538944 | tf_op jit(solution)/shard_map/reduce_scatter | solution.py:215
  56.4 3.2 %copy-start.7 = (bf16[768,2048]{1,0:T(8,128)(2,1)S(1)}, bf16[768,2048]{1,0:T(8,128)(2,1)}, u32[]{:S(2)}) copy-start(bf16[768,2048]{1,0:T(8,128)(2,1)} %all-gather.3.cloned.1.call-done) | copy-start | bytes 9437188
  56.4 3.2 %copy-start.16 = (f32[768]{0:T(1024)S(1)}, f32[768]{0:T(1024)}, u32[]{:S(2)}) copy-start(f32[768]{0:T(1024)} %copy-done.15) | copy-start | bytes 9220
  56.4 3.2 %copy-start.20 = (bf16[2048,64]{0,1:T(8,128)(2,1)S(1)}, bf16[2048,64]{0,1:T(8,128)(2,1)}, u32[]{:S(2)}) copy-start(bf16[2048,64]{0,1:T(8,128)(2,1)} %param.21) | copy-start | bytes 786436
  56.4 3.2 %copy-start.25 = (f32[2048]{0:T(1024)S(1)}, f32[2048]{0:T(1024)}, u32[]{:S(2)}) copy-start(f32[2048]{0:T(1024)} %param.19) | copy-start | bytes 24580
  61.4 12.1 %collective-permute-start = (bf16[128,128]{0,1:T(8,128)(2,1)}, bf16[128,128]{0,1:T(8,128)(2,1)}, u32[]{:S(2)}, u32[]{:S(2)}) collective-permute-start(bf16[128,128]{0,1:T(8,128)(2,1)} %get-tuple-element.120), channel_id=1, source_target_pairs={{0,8},{8,16},{16,24},{24,32},{32,40},{40,48},{48,56},{56,64},{64,7... | collective-permute-start | bytes 98312 | tf_op jit(solution)/shard_map/ppermute | solution.py:28
  65.1 4.4 %copy-start.19 = (bf16[768,192]{0,1:T(8,128)(2,1)S(1)}, bf16[768,192]{0,1:T(8,128)(2,1)}, u32[]{:S(2)}) copy-start(bf16[768,192]{0,1:T(8,128)(2,1)} %param.29) | copy-start | bytes 884740
  65.1 4.5 %copy-start.26 = (f32[768]{0:T(1024)S(1)}, f32[768]{0:T(1024)}, u32[]{:S(2)}) copy-start(f32[768]{0:T(1024)} %param.27) | copy-start | bytes 9220
  65.1 5.0 %copy-start.13 = (f32[768,16]{0,1:T(8,128)S(1)}, f32[768,16]{0,1:T(8,128)}, u32[]{:S(2)}) copy-start(f32[768,16]{0,1:T(8,128)} %get-tuple-element.124) | copy-start | bytes 147460
  65.1 5.0 %copy-start.14 = (f32[768,16]{0,1:T(8,128)S(1)}, f32[768,16]{0,1:T(8,128)}, u32[]{:S(2)}) copy-start(f32[768,16]{0,1:T(8,128)} %get-tuple-element.125) | copy-start | bytes 147460
  65.1 5.1 %copy-start.18 = (bf16[2048,128]{1,0:T(8,128)(2,1)S(1)}, bf16[2048,128]{1,0:T(8,128)(2,1)}, u32[]{:S(2)}) copy-start(bf16[2048,128]{1,0:T(8,128)(2,1)} %param.20) | copy-start | bytes 1572868
  65.1 8.4 %collective-permute-start.1 = (bf16[128,128]{0,1:T(8,128)(2,1)}, bf16[128,128]{0,1:T(8,128)(2,1)}, u32[]{:S(2)}, u32[]{:S(2)}) collective-permute-start(bf16[128,128]{0,1:T(8,128)(2,1)} %get-tuple-element.121), channel_id=1, source_target_pairs={{8,0},{16,8},{24,16},{32,24},{40,32},{48,40},{56,48},{64,56},{72,6... | collective-permute-start | bytes 98312 | tf_op jit(solution)/shard_map/ppermute | solution.py:29
  70.2 3.3 %copy-start.10 = (bf16[768,64]{0,1:T(8,128)(2,1)S(1)}, bf16[768,64]{0,1:T(8,128)(2,1)}, u32[]{:S(2)}) copy-start(bf16[768,64]{0,1:T(8,128)(2,1)} %copy-done.9) | copy-start | bytes 294916
  70.2 3.3 %copy-start.12 = (bf16[768,64]{0,1:T(8,128)(2,1)S(1)}, bf16[768,64]{0,1:T(8,128)(2,1)}, u32[]{:S(2)}) copy-start(bf16[768,64]{0,1:T(8,128)(2,1)} %copy-done.11) | copy-start | bytes 294916
  125.3 8.7 %slice-start = ((bf16[12288,288]{0,1:T(8,128)(2,1)}), bf16[12288,32]{0,1:T(8,128)(2,1)S(1)}, s32[]{:S(2)}) async-start(bf16[12288,288]{0,1:T(8,128)(2,1)} %all-gather.5.cloned.1.call-done), calls=%async_computation.4 | async-start | bytes 1572864 | tf_op jit(solution)/shard_map/slice | solution.py:38
  200.6 38.6 %copy-start.1 = (bf16[2048,768]{1,0:T(8,128)(2,1)S(1)}, bf16[2048,768]{1,0:T(8,128)(2,1)}, u32[]{:S(2)}) copy-start(bf16[2048,768]{1,0:T(8,128)(2,1)} %param.24) | copy-start | bytes 9437188
  (10 other events, 16.5 us)
Sparse Core Ops, SparseCore 0:
  9.0 34.7 all-gather.2
  53.9 65.2 all-gather.4
  206.5 32.6 reduce-scatter.1
where the time goes:
time: 249 us; the launch traced here: 246 us
  waiting for transfers between devices  106 us (43%)
  matrix products  65.2 us (26%)
  local copies, waits for them, and re-layouts  33.7 us (14%)
  other arithmetic  20.7 us (8%)
  between operations  13.6 us (5%)
  starting transfers between devices  5.37 us (2%)
    all_gather x1, waiting for transfers between devices, per_device(): lax.all_gather(tokens, 'tp', axis=1, tiled=True).astype(jnp.float32)  36.4 us
    all_gather x1, waiting for transfers between devices, side_by_side(): lax.all_gather(both, axis, axis=dim, tiled=True)  36.3 us
    reduce_scatter x1, waiting for transfers between devices, per_device(): lax.psum_scatter((jnp.dot(out_window, window_out, preferred_element_type=...  32.9 us
    dynamic_slice x24, local copies, waits for them, and re-layouts, in_blocks(): running, unused = lax.scan(scan_step, running, blocked)  15.4 us
    slice x4, local copies, waits for them, and re-layouts, side_by_side(): lax.slice_in_dim(whole, at, at + a.shape[along], axis=along)  14.8 us
    dot_general x12, matrix products, attend(): jnp.einsum('hqk,khd->qhd', weights.astype(jnp.bfloat16), value_rows, pref...  13.7 us
    dot_general x6, matrix products, per_device(): updated.append(jnp.dot(scaled, weight, preferred_element_type=jnp.float32))  12.6 us
    dot_general x12, matrix products, attend(): jnp.einsum('qhr,kr->hqk', q_rot, rot_keys, preferred_element_type=jnp.flo...  12.3 us
  transfers between devices with their start and end apart: 5, of which 3 were waited for; matrix products, arithmetic and copies ran while one was open for 10% of the time, Pallas kernels for 0%

commit v1 on v0

v1 whole, which is shorter than its diff:
```python
import functools
import jax
import jax.numpy as jnp
from jax import lax
from jax.experimental import pallas as pl
from jax.experimental.pallas import tpu as pltpu
from jax.sharding import PartitionSpec as P

WINDOW = 128
EPS = 1e-06
THETA = 10000.0
LOG2E = 1.4426950408889634
f32, bf16 = jnp.float32, jnp.bfloat16
MESH = pl.DeviceIdType.MESH
QT = 256
NEG = -1e30


def attention_kernel(
    rows, nz, nx,
    kvm, qt, qwt, kvw, heads,
    out,
    kvb, rotx, qb, kvp, mref, lref, acc, s00, s01, s10, s11, x00, x01, x10, x11,
    osend, ssend, obuf, sbuf,
    h_send, h_recv, q_send, q_recv, qf_send, qf_recv, k_send, k_recv, kf_send, kf_recv,
    o_send, o_recv, s_send, s_recv,
):
    sp = lax.axis_index("sp")
    tp = lax.axis_index("tp")
    z, x = sp // nx, sp % nx
    nsp = nz * nx
    tiles = rows // QT
    half = kvm.shape[0] // 2

    def at(zz, xx):
        return (zz * nx + xx, tp)

    xr, xl = at(z, (x + 1) % nx), at(z, (x + nx - 1) % nx)
    zr, zl, zo = at((z + 1) % nz, x), at((z + nz - 1) % nz, x), at((z + 2) % nz, x)
    nxt, prv = ((sp + 1) % nsp, tp), ((sp + nsp - 1) % nsp, tp)

    barrier = pltpu.get_barrier_semaphore()
    for peer in (xr, xl, zr, zl, zo, nxt, prv):
        pl.semaphore_signal(barrier, inc=1, device_id=peer, device_id_type=MESH)
    pl.semaphore_wait(barrier, 7)

    def remote(src, dst, ss, rs, dev):
        return pltpu.make_async_remote_copy(
            src_ref=src, dst_ref=dst, send_sem=ss, recv_sem=rs, device_id=dev, device_id_type=MESH
        )

    halo = [
        remote(kvw.at[pl.ds(rows - WINDOW, WINDOW)], kvp.at[pl.ds(0, WINDOW)], h_send.at[0], h_recv.at[0], nxt),
        remote(kvw.at[pl.ds(0, WINDOW)], kvp.at[pl.ds(rows + WINDOW, WINDOW)], h_send.at[1], h_recv.at[1], prv),
    ]
    q_out = {}
    for order in ((0, 1), (1, 0)):
        for which, h in ((0, order[0]), (1, order[1])):
            slot, dev = ((1, zr), (2, zl))[which]
            q_out[(which, h)] = remote(
                qt.at[h], qb.at[slot, h], q_send.at[which, h], q_recv.at[which, h], dev
            )
    k_out = {}
    for order in ((0, 1), (1, 0)):
        for which, h in ((0, order[0]), (1, order[1])):
            slot, dev = ((1, xr), (2, xl))[which]
            k_out[(which, h)] = remote(
                kvm.at[pl.ds(h * half, half)], kvb.at[slot, pl.ds(h * half, half)],
                k_send.at[which, h], k_recv.at[which, h], dev,
            )
    for c in halo:
        c.start()
    for key in ((0, 0), (1, 1), (0, 1), (1, 0)):
        q_out[key].start()
        k_out[key].start()
    q_fwd = [
        remote(qb.at[1, 0], qb.at[3, 0], qf_send.at[0], qf_recv.at[0], zr),
        remote(qb.at[2, 1], qb.at[3, 1], qf_send.at[1], qf_recv.at[1], zl),
    ]
    k_fwd = [
        remote(kvb.at[1, pl.ds(0, half)], kvb.at[3, pl.ds(0, half)], kf_send.at[0], kf_recv.at[0], xr),
        remote(kvb.at[2, pl.ds(half, half)], kvb.at[3, pl.ds(half, half)], kf_send.at[1], kf_recv.at[1], xl),
    ]

    mref[...] = jnp.full(mref.shape, NEG, f32)
    lref[...] = jnp.zeros(lref.shape, f32)
    acc[...] = jnp.zeros(acc.shape, f32)
    ssend[...] = jnp.zeros(ssend.shape, f32)
    qb[0] = qt[...]
    kvb[0] = kvm[...]
    kvp[WINDOW : WINDOW + rows] = kvw[...]
    quarter = rows // 4

    def unpack(i):
        packed = kvb[i, rows : rows + quarter].astype(f32)
        for g in range(4):
            moved = packed if g == 0 else pltpu.roll(packed, 128 - 32 * g, 1)
            rotx[i, g * quarter : (g + 1) * quarter] = moved.astype(bf16)

    S = ((s00, s01), (s10, s11))
    X = ((x00, x01), (x10, x11))

    def stage_a(k, q, t, slot):
        z64, z96 = jnp.zeros((64, QT), bf16), jnp.zeros((96, QT), bf16)
        keys = jnp.concatenate([kvb[k, 0:rows], rotx[k]], axis=1)
        for h in range(2):
            qq = qb[q, h, t]
            if h == 0:
                parts = [qq[0:64], z64, qq[64:96], z96]
            else:
                parts = [z64, qq[0:64], qq[64:96], z96]
            s = jnp.dot(keys, jnp.concatenate(parts, axis=0), preferred_element_type=f32)
            S[slot][h][...] = s
            X[slot][h][...] = jnp.max(s.reshape(rows // 8, 8, QT), axis=0)

    def stage_b(k, q, t, slot):
        for h in range(2):
            old = mref[q, t, h : h + 1]
            new = jnp.maximum(old, jnp.max(X[slot][h][...], axis=0, keepdims=True))
            alpha = jnp.exp2(old - new)
            mref[q, t, h : h + 1] = new
            total = None
            for c in range(rows // 256):
                p = jnp.exp2(S[slot][h][c * 256 : (c + 1) * 256] - new).astype(bf16)
                base = rows + quarter + 256 * c + 64 * h
                v = jnp.concatenate([kvb[k, base : base + 64], kvb[k, base + 128 : base + 192]], axis=1)
                v = jnp.concatenate([v, jnp.ones((16, 256), bf16)], axis=0)
                o = jnp.dot(v, p, preferred_element_type=f32)
                total = o if total is None else total + o
            lref[q, t, h : h + 1] = lref[q, t, h : h + 1] * alpha + total[64:65]
            acc[q, t, 64 * h : 64 * h + 64] = acc[q, t, 64 * h : 64 * h + 64] * alpha + total[0:64]

    def pipeline(n, where, before=None):
        def A(i, slot):
            stage_a(*where(i), slot)

        def B(i, slot):
            stage_b(*where(i), slot)

        A(0, 0)
        loops = (n - 1) // 2

        @pl.loop(0, loops)
        def _(j):
            i = 2 * j
            if before is not None:
                before(i + 1)
            A(i + 1, 1)
            B(i, 0)
            if before is not None:
                before(i + 2)
            A(i + 2, 0)
            B(i + 1, 1)

        i = 2 * loops
        if n % 2 == 0:
            if before is not None:
                before(i + 1)
            A(i + 1, 1)
            B(i, 0)
            B(i + 1, 1)
        else:
            B(i, 0)

    def window():
        for c in halo:
            c.wait_recv()
        span = QT + 2 * WINDOW
        key_i = lax.broadcasted_iota(jnp.int32, (span, QT), 0)
        dist = key_i - WINDOW - lax.broadcasted_iota(jnp.int32, (span, QT), 1)
        dist = jnp.abs(dist)
        distf = dist.astype(f32)

        @pl.loop(0, tiles)
        def _(t):
            rows_at = pl.ds(pl.multiple_of(t * QT, QT), span)
            kv = kvp[rows_at]
            pos = sp * rows + t * QT + key_i - WINDOW
            valid = (dist <= WINDOW) & (pos >= 0) & (pos < nsp * rows)
            for h in range(2):
                slope, sink = heads[0, h], heads[1, h]
                rhs = jnp.concatenate([qwt[t, h], jnp.zeros((64, QT), bf16)], axis=0)
                s = jnp.dot(kv, rhs, preferred_element_type=f32) * 0.125
                s = jnp.where(valid, s - slope * distf, NEG)
                m = jnp.maximum(jnp.max(s, axis=0, keepdims=True), sink)
                w = jnp.exp2((s - m) * LOG2E)
                denom = jnp.sum(w, axis=0, keepdims=True) + jnp.exp2((sink - m) * LOG2E)
                w = (w * (1.0 / denom)).astype(bf16)
                o = lax.dot_general(kv, w, (((0,), (0,)), ((), ())), preferred_element_type=f32)
                S[0][0][h * 64 : h * 64 + 64] = o[64:128]
            out[pl.ds(pl.multiple_of(t * QT, QT), QT), 0:128] = S[0][0][0:128].T.astype(bf16)

    unpack(0)

    @pl.loop(0, 3)
    def _(q):
        @pl.when(q == 1)
        def _():
            window()
            for c, f in ((q_out[(0, 0)], q_fwd[0]), (q_out[(1, 1)], q_fwd[1])):
                c.wait_recv()
                f.start()
            q_out[(0, 1)].wait_recv()

        @pl.when(q == 2)
        def _():
            q_out[(1, 0)].wait_recv()
            for c, f in ((k_out[(0, 0)], k_fwd[0]), (k_out[(1, 1)], k_fwd[1])):
                c.wait_recv()
                f.start()

        pipeline(tiles, lambda i: (0, q, i))

    k_out[(0, 1)].wait_recv()
    k_out[(1, 0)].wait_recv()
    unpack(1)
    unpack(2)
    for c in q_fwd:
        c.wait_recv()

    def arrive(i):
        @pl.when(i == 3 * tiles)
        def _():
            for c in k_fwd:
                c.wait_recv()
            unpack(3)

    def finish(q):
        for t in range(tiles):
            for h in range(2):
                inv = 1.0 / lref[q, t, h : h + 1]
                osend[q, t, 64 * h : 64 * h + 64] = (acc[q, t, 64 * h : 64 * h + 64] * inv).astype(bf16)
            ssend[q, t, 0:2] = mref[q, t, 0:2]
            ssend[q, t, 2:4] = lref[q, t, 0:2]

    back = {}
    for q, slot, dev in ((3, 3, zo), (2, 1, zr), (1, 2, zl)):
        back[q] = (
            remote(osend.at[q], obuf.at[slot], o_send.at[q], o_recv.at[slot], dev),
            remote(ssend.at[q], sbuf.at[slot], s_send.at[q], s_recv.at[slot], dev),
        )

    pipeline(4 * tiles, lambda i: (i // tiles, 3, i % tiles), arrive)
    finish(3)
    for c in back[3]:
        c.start()

    @pl.loop(0, 3)
    def _(r):
        q = 2 - r
        pipeline(3 * tiles, lambda i: (1 + i // tiles, q, i % tiles))
        finish(q)
        for n in (0, 1):
            @pl.when(r == n)
            def _():
                for c in back[2 - n]:
                    c.start()

    for q in (3, 2, 1):
        for c in back[q]:
            c.wait_recv()

    @pl.loop(0, tiles)
    def _(t):
        ms = [ssend[0, t, 0:2]] + [sbuf[j, t, 0:2] for j in (1, 2, 3)]
        ls = [ssend[0, t, 2:4]] + [sbuf[j, t, 2:4] for j in (1, 2, 3)]
        top = jnp.maximum(jnp.maximum(ms[0], ms[1]), jnp.maximum(ms[2], ms[3]))
        ws = [l * jnp.exp2(m - top) for m, l in zip(ms, ls)]
        inv = 1.0 / (ws[0] + ws[1] + ws[2] + ws[3])
        for h in range(2):
            rows_h = slice(64 * h, 64 * h + 64)
            total = osend[0, t, rows_h].astype(f32) * (ws[0] * inv)[h : h + 1]
            for j in (1, 2, 3):
                total = total + obuf[j, t, rows_h].astype(f32) * (ws[j] * inv)[h : h + 1]
            S[0][0][rows_h] = total
        out[pl.ds(pl.multiple_of(t * QT, QT), QT), 128:256] = S[0][0][0:128].T.astype(bf16)

    for c in halo + list(q_out.values()) + list(k_out.values()) + q_fwd + k_fwd:
        c.wait_send()
    for q in (3, 2, 1):
        for c in back[q]:
            c.wait_send()


def attention(kvm, qt, qwt, kvw, heads, rows, nz, nx):
    tiles = rows // QT
    dma = pltpu.SemaphoreType.DMA
    V = pltpu.VMEM
    vm = pl.BlockSpec(memory_space=pltpu.VMEM)
    return pl.pallas_call(
        functools.partial(attention_kernel, rows, nz, nx),
        out_shape=jax.ShapeDtypeStruct((rows, 256), bf16),
        in_specs=[vm, vm, vm, vm, pl.BlockSpec(memory_space=pltpu.SMEM)],
        out_specs=vm,
        scratch_shapes=[
            V((4,) + kvm.shape, bf16), V((4, rows, 128), bf16), V((4, 2, tiles, 96, QT), bf16),
            V((rows + 2 * WINDOW, 128), bf16),
            V((4, tiles, 8, QT), f32), V((4, tiles, 8, QT), f32), V((4, tiles, 128, QT), f32),
        ]
        + [V((rows, QT), f32)] * 4 + [V((8, QT), f32)] * 4
        + [
            V((4, tiles, 128, QT), bf16), V((4, tiles, 8, QT), f32),
            V((4, tiles, 128, QT), bf16), V((4, tiles, 8, QT), f32),
            dma((2,)), dma((2,)), dma((2, 2)), dma((2, 2)), dma((2,)), dma((2,)),
            dma((2, 2)), dma((2, 2)), dma((2,)), dma((2,)),
            dma((4,)), dma((4,)), dma((4,)), dma((4,)),
        ],
        compiler_params=pltpu.CompilerParams(
            collective_id=1, has_side_effects=True, vmem_limit_bytes=48 * 2**20
        ),
        name="attention",
    )(kvm, qt, qwt, kvw, heads)


def rotate(vector, positions):
    half_len = vector.shape[-1] // 2
    inverse = THETA ** (-jnp.arange(half_len, dtype=f32) / half_len)
    angles = positions.astype(f32)[:, None] * inverse[None, :]
    new_shape = (angles.shape[0],) + (1,) * (vector.ndim - 2) + (half_len,)
    cosine, sine = jnp.cos(angles).reshape(new_shape), jnp.sin(angles).reshape(new_shape)
    a, b = vector[..., :half_len].astype(f32), vector[..., half_len:].astype(f32)
    return jnp.concatenate([a * cosine - b * sine, b * cosine + a * sine], axis=-1)


def norm_rows(values, gain):
    v = values.astype(f32)
    return (v * lax.rsqrt(jnp.mean(v * v, axis=1, keepdims=True) + EPS) * gain).astype(bf16)


def per_device(
    tokens, norm_gain, window_query, window_key, window_value, sink_logit, down_query, down_latent,
    rotary_proj, query_gain, latent_gain, up_query, up_key, up_value, window_out, latent_out,
):
    rows = tokens.shape[0]
    tiles = rows // QT
    width = tokens.shape[1] * lax.axis_size("tp")
    as_float = lax.all_gather(tokens, "tp", axis=1, tiled=True).astype(f32)
    scaled = (as_float * norm_gain[None, :]).astype(bf16)
    row_scale = lax.rsqrt(jnp.sum(as_float * as_float, axis=1) / width + EPS)[:, None]

    def project(weight):
        return (jnp.dot(scaled, weight, preferred_element_type=f32) * row_scale).astype(bf16)

    latent_kv, rotary_rows = project(down_latent), project(rotary_proj)
    q_window, k_window, v_window = project(window_query), project(window_key), project(window_value)
    latent_q = project(down_query)
    positions = lax.axis_index("sp") * rows + jnp.arange(rows, dtype=jnp.int32)
    k_rot = rotate(rotary_rows, positions).astype(bf16)
    normed_kv = norm_rows(latent_kv, latent_gain)
    keys = jnp.dot(normed_kv, up_key, preferred_element_type=f32).astype(bf16)
    values = jnp.dot(normed_kv, up_value, preferred_element_type=f32).astype(bf16)
    quarter = rows // 4
    rot4 = jnp.concatenate([k_rot[g * quarter : (g + 1) * quarter] for g in range(4)], axis=1)
    vt = values.reshape(rows // 128, 128, 128).transpose(0, 2, 1).reshape(rows, 128)
    kvm = jnp.concatenate([keys, rot4, vt], axis=0)
    q = jnp.dot(norm_rows(latent_q, query_gain), up_query, preferred_element_type=f32)
    q = (q * (LOG2E * 96 ** (-0.5))).reshape(rows, 2, 96)
    q = jnp.concatenate([q[..., :64], rotate(q[..., 64:], positions)], axis=-1).astype(bf16)
    qt = q.reshape(tiles, QT, 2, 96).transpose(2, 0, 3, 1)
    qwt = q_window.reshape(tiles, QT, 2, 64).transpose(0, 2, 3, 1)
    kvw = jnp.concatenate([k_window, v_window], axis=1)
    head_ids = (lax.axis_index("tp") * 2 + jnp.arange(2)).astype(f32)
    heads = jnp.stack([jnp.exp2(-8.0 * (head_ids + 1.0) / 16), sink_logit])
    nsp = lax.axis_size("sp")
    nx = 4
    mixed_in = attention(kvm, qt, qwt, kvw, heads, rows, nsp // nx, nx)
    out_rows = jnp.concatenate([window_out, latent_out], axis=0)
    part = jnp.dot(mixed_in, out_rows, preferred_element_type=f32).astype(bf16)
    return lax.psum_scatter(part, "tp", scatter_dimension=0, tiled=True)


def solution(mesh):
    col, row, rep = P(None, "tp"), P("tp", None), P()
    placed = (
        P("sp", "tp"), rep, col, col, col, P("tp"), rep, rep, rep, rep, rep, col, col, col, row, row,
    )
    return jax.shard_map(
        per_device, mesh=mesh, in_specs=placed, out_specs=P(("sp", "tp"), None), check_vma=False
    )
```

time: 249 us -> 157 us (0.63)
  matrix products: 65.2 us -> 20.1 us
  Pallas kernels: 0 us -> 37.5 us
  waiting for transfers between devices: 106 us -> 70.1 us
  local copies, waits for them, and re-layouts: 33.7 us -> 6.86 us
  other arithmetic: 20.7 us -> 5.99 us
  starting transfers between devices: 5.37 us -> 0.04 us
    dot_general x48 -> x9, matrix products: 64.6 us -> 19.5 us  [the longest x6 15.1 us: project(): jnp.dot(scaled, weight, preferred_element_type=f32) * row_scale]
    pallas_call x0 -> x1, Pallas kernels: none -> 37.5 us  [attention(): pl.pallas_call(functools.partial(attention_kernel, rows, nz, nx), out_sha...]
    all_gather x2 -> x1, waiting for transfers between devices: 72.7 us -> 35.6 us  [per_device(): as_float = lax.all_gather(tokens, 'tp', axis=1, tiled=True).astype(f32)]
    slice x17 -> x1, local copies, waits for them, and re-layouts: 16 us -> 0.02 us  [per_device(): q[..., :64]]
    dynamic_slice x24 -> x0, local copies, waits for them, and re-layouts: 15.4 us -> none  [in_blocks(): running, unused = lax.scan(scan_step, running, blocked)]
    reduce_sum x14 -> x1, other arithmetic: 13.6 us -> 2.72 us  [per_device(): jnp.sum(as_float * as_float, axis=1) / width + EPS]
    ppermute x2 -> x0, starting transfers between devices: 5.29 us -> none  [the longest x1 3.68 us: with_halo(): before = lax.ppermute(last, axis, up)]
    reshape x1 -> x3, local copies, waits for them, and re-layouts: 0.06 us -> 3 us  [the longest x2 2.18 us: per_device(): qwt = q_window.reshape(tiles, QT, 2, 64).transpose(0, 2, 3, 1)]
  transfers between devices with their start and end apart: 5 -> 2, of which waited for: 3 -> 2; matrix products, arithmetic and copies ran while one was open for 10% -> 1% of each run, Pallas kernels for 0% -> 0%
where the time goes in v1:
time: 157 us; the launch traced here: 154 us
  waiting for transfers between devices  70.1 us (45%)
  Pallas kernels  37.5 us (24%)
  matrix products  20.1 us (13%)
  between operations  13.8 us (9%)
  local copies, waits for them, and re-layouts  6.86 us (4%)
  other arithmetic  5.99 us (4%)
    pallas_call x1, Pallas kernels, attention(): pl.pallas_call(functools.partial(attention_kernel, rows, nz, nx), out_sha...  37.5 us
    all_gather x1, waiting for transfers between devices, per_device(): as_float = lax.all_gather(tokens, 'tp', axis=1, tiled=True).astype(f32)  35.6 us
    reduce_scatter x1, waiting for transfers between devices, per_device(): return lax.psum_scatter(part, 'tp', scatter_dimension=0, tiled=True)  33.7 us
    dot_general x6, matrix products, project(): jnp.dot(scaled, weight, preferred_element_type=f32) * row_scale  15.1 us
    unnamed x44, local copies, waits for them, and re-layouts  3.82 us
  transfers between devices with their start and end apart: 2, of which 2 were waited for; matrix products, arithmetic and copies ran while one was open for 1% of the time, Pallas kernels for 0%

profile of v1, /device:TPU:1, one launch (start us, length us, event | category | flops | bytes accessed | tf_op | source)
XLA Modules:
  0.0 154.3 jit_solution(14778788215623644140)
XLA Ops:
  6.5 0.7 all-gather.2.cloned.1.call-update
  7.3 0.8 pad_maximum_fusion.3.heads
  8.2 35.6 %all-gather.2.cloned.1.call-done = bf16[768,2048]{1,0:T(8,128)(2,1)} async-done(((bf16[768,256]{1,0:T(8,128)(2,1)}), bf16[768,2048]{1,0:T(8,128)(2,1)}) %all-gather.2.cloned.1.call-update) | async-done | bytes 3145744 | tf_op jit(solution)/shard_map/all_gather | solution.py:337
  43.8 2.7 %fusion.1 = f32[768]{0:T(1024)S(1)} fusion(bf16[768,2048]{1,0:T(8,128)(2,1)} %all-gather.2.cloned.1.call-done), kind=kLoop, calls=%fused_computation.3 | loop fusion | flops 4717824 | bytes 3148800 | tf_op jit(solution)/shard_map/reduce_sum | solution.py:339
  46.6 2.8 %fusion.2 = (f32[768]{0:T(1024)S(1)}, bf16[768,768]{0,1:T(8,128)(2,1)S(1)}) fusion(f32[768]{0:T(1024)S(1)} %add_rsqrt_fusion.2, bf16[2048,768]{1,0:T(8,128)(2,1)S(1)} %copy-done, bf16[768,2048]{1,0:T(8,128)(2,1)S(1)} %copy-done.1, f32[2048]{0:T(1024)S(1)} %copy-done.17), kind=kOutput, calls=%fused_computation.7 | convolution fusion | flops 2423586048 | bytes 7485440 | tf_op jit(solution)/shard_map/dot_general | solution.py:342
  50.1 0.8 copy-done.6
  50.9 1.0 fusion.42
  51.9 0.9 multiply_cosine_fusion
  52.9 0.7 copy.60
  53.7 0.7 copy.61
  54.4 0.7 copy.62
  55.1 0.7 copy.63
  55.8 4.5 %fusion.5 = (f32[768]{0:T(1024)S(1)}, bf16[768,512]{0,1:T(8,128)(2,1)S(1)}) fusion(f32[768]{0:T(1024)S(1)} %add_rsqrt_fusion.2, bf16[2048,512]{1,0:T(8,128)(2,1)} %param.23, bf16[768,2048]{1,0:T(8,128)(2,1)} %all-gather.2.cloned.1.call-done, f32[2048]{0:T(1024)S(1)} %copy-done.17), kind=kOutput, calls=%fused_computation.13 | convolution fusion | flops 1617296640 | bytes 6043648 | tf_op jit(solution)/shard_map/dot_general | solution.py:342
  60.3 1.2 convolution_convert_fusion.2
  62.1 0.8 copy.46
  62.9 3.0 %fusion.36 = bf16[768,128]{1,0:T(8,128)(2,1)S(1)} fusion(bf16[2048,128]{1,0:T(8,128)(2,1)} %param.18, bf16[768,2048]{1,0:T(8,128)(2,1)} %all-gather.2.cloned.1.call-done, f32[2048]{0:T(1024)S(1)} %copy-done.17, f32[768]{0:T(1024)S(1)} %add_rsqrt_fusion.2), kind=kOutput, calls=%fused_computation.29 | convolution fusion | flops 407568384 | bytes 3877888 | tf_op jit(solution)/shard_map/dot_general | solution.py:342
  65.9 0.9 reshape.126
  66.8 1.2 copy.51
  68.1 1.1 subtract_convert_fusion
  69.3 2.9 %fusion.30 = bf16[768,64]{1,0:T(8,128)(2,1)S(1)} fusion(bf16[2048,64]{0,1:T(8,128)(2,1)} %param.20, bf16[768,2048]{1,0:T(8,128)(2,1)} %all-gather.2.cloned.1.call-done, f32[2048]{0:T(1024)S(1)} %copy-done.17, f32[768]{0:T(1024)S(1)} %add_rsqrt_fusion.2), kind=kOutput, calls=%fused_computation.27 | convolution fusion | flops 206143488 | bytes 3517440 | tf_op jit(solution)/shard_map/dot_general | solution.py:342
  72.2 1.0 fusion.33
  73.5 37.5 %attention.1 = bf16[768,256]{1,0:T(8,128)(2,1)S(1)} custom-call(bf16[1728,128]{1,0:T(8,128)(2,1)S(1)} %pad_maximum_fusion.kvm, bf16[2,3,96,256]{3,2,1,0:T(8,128)(2,1)S(1)} %maximum_bitcast_fusion.qt, bf16[3,2,64,256]{3,2,1,0:T(8,128)(2,1)S(1)} %bitcast.29, bf16[768,128]{1,0:T(8,128)(2,1)S(1)} %pad_maximum_fusion.1.kvw, f32[2,2]{1,0:T(2,128)S(1)} %pad_maximum_fusion.3.heads), custom_call_target="tpu_custom_call" | custom-call | tf_op jit(solution)/shard_map/attention/pallas_call | solution.py:290
  111.1 2.6 %convolution_convert_fusion = bf16[768,2048]{1,0:T(8,128)(2,1)} fusion(bf16[768,256]{1,0:T(8,128)(2,1)S(1)} %attention.1, bf16[128,2048]{1,0:T(8,128)(2,1)S(1)} %copy-done.4, bf16[128,2048]{1,0:T(8,128)(2,1)S(1)} %copy-done.5), kind=kOutput, calls=%fused_computation.4 | convolution fusion | flops 808976384 | bytes 4587520 | tf_op jit(solution)/shard_map/dot_general | solution.py:368
  113.7 33.7 %reduce-scatter.2.cloned.1.call-done = bf16[96,2048]{1,0:T(8,128)(2,1)} async-done(((bf16[768,2048]{1,0:T(8,128)(2,1)}), bf16[96,2048]{1,0:T(8,128)(2,1)}) %reduce-scatter.2.cloned.1.call-update) | async-done | bytes 393232 | tf_op jit(solution)/shard_map/reduce_scatter | solution.py:369
  (57 shorter events, 1.8 us)
Async XLA Ops:
  6.5 40.0 %copy-start = (bf16[2048,768]{1,0:T(8,128)(2,1)S(1)}, bf16[2048,768]{1,0:T(8,128)(2,1)}, u32[]{:S(2)}) copy-start(bf16[2048,768]{1,0:T(8,128)(2,1)} %param.22) | copy-start | bytes 9437188
  6.5 40.0 %copy-start.17 = (f32[2048]{0:T(1024)S(1)}, f32[2048]{0:T(1024)}, u32[]{:S(2)}) copy-start(f32[2048]{0:T(1024)} %param.17) | copy-start | bytes 24580
  6.5 37.2 %all-gather.2.cloned.1.call-start = ((), (), s32[]{:S(2)}) async-start(), calls=%async_computation.1 | async-start | bytes 3538944 | tf_op jit(solution)/shard_map/all_gather | solution.py:337
  7.3 140.2 %reduce-scatter.2.cloned.1.call-start = ((), (), s32[]{:S(2)}) async-start(), calls=%async_computation.2 | async-start | bytes 3538944 | tf_op jit(solution)/shard_map/reduce_scatter | solution.py:369
  43.8 2.8 %copy-start.1 = (bf16[768,2048]{1,0:T(8,128)(2,1)S(1)}, bf16[768,2048]{1,0:T(8,128)(2,1)}, u32[]{:S(2)}) copy-start(bf16[768,2048]{1,0:T(8,128)(2,1)} %all-gather.2.cloned.1.call-done) | copy-start | bytes 9437188
  46.6 2.8 %copy-start.12 = (bf16[768,192]{0,1:T(8,128)(2,1)S(1)}, bf16[768,192]{0,1:T(8,128)(2,1)}, u32[]{:S(2)}) copy-start(bf16[768,192]{0,1:T(8,128)(2,1)} %param.27) | copy-start | bytes 884740
  46.6 2.8 %copy-start.18 = (f32[768]{0:T(1024)S(1)}, f32[768]{0:T(1024)}, u32[]{:S(2)}) copy-start(f32[768]{0:T(1024)} %param.25) | copy-start | bytes 9220
  49.4 1.5 copy-start.14
  50.0 0.8 copy-start.6
  55.8 4.5 %copy-start.15 = (bf16[512,128]{1,0:T(8,128)(2,1)S(1)}, bf16[512,128]{1,0:T(8,128)(2,1)}, u32[]{:S(2)}) copy-start(bf16[512,128]{1,0:T(8,128)(2,1)} %param.28) | copy-start | bytes 393220
  55.8 4.5 %copy-start.19 = (f32[512]{0:T(512)S(1)}, f32[512]{0:T(512)}, u32[]{:S(2)}) copy-start(f32[512]{0:T(512)} %param.26) | copy-start | bytes 6148
  55.8 5.7 %copy-start.16 = (bf16[512,128]{1,0:T(8,128)(2,1)S(1)}, bf16[512,128]{1,0:T(8,128)(2,1)}, u32[]{:S(2)}) copy-start(bf16[512,128]{1,0:T(8,128)(2,1)} %param.29) | copy-start | bytes 393220
  68.1 4.0 %copy-start.2 = (bf16[768,2048]{1,0:T(8,128)(2,1)S(1)}, bf16[768,2048]{1,0:T(8,128)(2,1)}, u32[]{:S(2)}) copy-start(bf16[768,2048]{1,0:T(8,128)(2,1)} %all-gather.2.cloned.1.call-done) | copy-start | bytes 9437188
  68.1 4.0 %copy-start.13 = (bf16[2048,64]{0,1:T(8,128)(2,1)S(1)}, bf16[2048,64]{0,1:T(8,128)(2,1)}, u32[]{:S(2)}) copy-start(bf16[2048,64]{0,1:T(8,128)(2,1)} %param.19) | copy-start | bytes 786436
  72.1 1.2 copy-start.3
  72.2 1.2 copy-start.7
  72.2 1.2 copy-start.8
  72.2 1.2 copy-start.9
  72.2 1.2 copy-start.10
  72.2 1.2 copy-start.11
  73.2 37.9 %copy-start.4 = (bf16[128,2048]{1,0:T(8,128)(2,1)S(1)}, bf16[128,2048]{1,0:T(8,128)(2,1)}, u32[]{:S(2)}) copy-start(bf16[128,2048]{1,0:T(8,128)(2,1)} %param.31) | copy-start | bytes 1572868
  73.2 37.9 %copy-start.5 = (bf16[128,2048]{1,0:T(8,128)(2,1)S(1)}, bf16[128,2048]{1,0:T(8,128)(2,1)}, u32[]{:S(2)}) copy-start(bf16[128,2048]{1,0:T(8,128)(2,1)} %param.30) | copy-start | bytes 1572868
Sparse Core Ops, SparseCore 0:
  9.0 34.7 all-gather.1
  113.9 33.5 reduce-scatter.1

commit v2 on v1

v2 whole, which is shorter than its diff:
```python
import functools
import jax
import jax.numpy as jnp
import numpy as np
from jax import lax
from jax.experimental import pallas as pl
from jax.experimental.pallas import tpu as pltpu
from jax.sharding import PartitionSpec as P

D = 2048
A_HEADS = 16
WINDOW = 128
EPS = 1e-06
THETA = 10000.0
LOG2E = 1.4426950408889634
f32, bf16 = jnp.float32, jnp.bfloat16
MESH = pl.DeviceIdType.MESH
QT = 256
NEG = -1e30
NX = 4


def remote(src, dst, ss, rs, dev):
    return pltpu.make_async_remote_copy(
        src_ref=src, dst_ref=dst, send_sem=ss, recv_sem=rs, device_id=dev, device_id_type=MESH
    )


class ChipGather:
    def __init__(self, own, buf, core, right, left, partner, sems):
        ysend, yrecv, fsend, psend, precv = sems
        self.own, self.buf, self.core = own, buf, core
        self.out = {
            (s, p): remote(own[p], buf.at[s, core, p], ysend.at[s, p], yrecv.at[s, p], dev)
            for s, dev in ((1, right), (2, left))
            for p in (0, 1)
        }
        self.fwd = {
            (3, 0): remote(buf.at[1, core, 0], buf.at[3, core, 0], fsend.at[0], yrecv.at[3, 0], right),
            (3, 1): remote(buf.at[2, core, 1], buf.at[3, core, 1], fsend.at[1], yrecv.at[3, 1], left),
        }
        self.relay = {
            (s, p): remote(
                own[p] if s == 0 else buf.at[s, core, p], buf.at[s, core, p],
                psend.at[s, p], precv.at[s, p], partner,
            )
            for s in range(4)
            for p in (0, 1)
        }

    def start(self):
        for key in ((1, 0), (2, 1), (1, 1), (2, 0)):
            self.out[key].start()
        for p in (0, 1):
            self.relay[(0, p)].start()

    def arrive(self, slot, part, relay=True):
        (self.fwd if slot == 3 else self.out)[(slot, part)].wait_recv()
        if (slot, part) == (1, 0):
            self.fwd[(3, 0)].start()
        if (slot, part) == (2, 1):
            self.fwd[(3, 1)].start()
        if relay:
            self.relay[(slot, part)].start()

    def partner(self, slot, part):
        self.relay[(slot, part)].wait_recv()

    def drain(self):
        for c in list(self.out.values()) + list(self.fwd.values()) + list(self.relay.values()):
            c.wait_send()


def layer_kernel(
    rows, nz, nx, ny,
    tokens, norm_gain, query_gain, latent_gain, sinks, slopes,
    w_query, w_key, w_value, d_query, d_latent, w_rot, u_query, u_key, u_value, o_window, o_latent,
    tab_far, tab_near,
    result,
    tb, wb, wdq, wdl, wcat, wk, wv, wr, uq, uk, uv, far, near, pacc, sq,
    kvm, qwt, kvw, osw, osl, orow,
    kvb, rotx, qb, kvp, mref, lref, acc, s00, s01, s10, s11, x00, x01, x10, x11,
    osend, ssend, obuf, sbuf,
    l_sem, t_ysend, t_yrecv, t_fsend, t_psend, t_precv, w_ysend, w_yrecv, w_fsend, w_psend, w_precv,
    a_send, a_recv,
    h_send, h_recv, q_send, q_recv, qf_send, qf_recv, k_send, k_recv, kf_send, kf_recv,
    o_send, o_recv, s_send, s_recv,
):
    sp = lax.axis_index("sp")
    tp = lax.axis_index("tp")
    z, x = sp // nx, sp % nx
    y, core = tp // 2, tp % 2
    nsp, ntp = nz * nx, ny * 2
    tiles = rows // QT
    half_rows = rows // 2
    mine = rows // ntp

    loads = [
        pltpu.make_async_copy(s, d, l_sem.at[i])
        for i, (s, d) in enumerate((
            (d_query, wdq), (d_latent, wdl), (w_query, wcat.at[:, pl.ds(0, 128)]), (w_key, wk),
            (w_value, wv), (w_rot, wr), (u_query, uq), (u_key, uk), (u_value, uv),
            (tab_far.at[sp], far), (tab_near, near),
            (o_window, wb.at[0, core, 0]), (o_latent, wb.at[0, core, 1]),
        ))
    ]
    for c in loads:
        c.start()

    def at(zz, xx):
        return (zz * nx + xx, tp)

    def chip(step, cc):
        return (sp, ((y + step) % ny) * 2 + cc)

    xr, xl = at(z, (x + 1) % nx), at(z, (x + nx - 1) % nx)
    zr, zl, zo = at((z + 1) % nz, x), at((z + nz - 1) % nz, x), at((z + 2) % nz, x)
    nxt, prv = ((sp + 1) % nsp, tp), ((sp + nsp - 1) % nsp, tp)
    partner = chip(0, 1 - core)
    others = [chip(d, cc) for d in range(1, ny) for cc in (0, 1)] + [partner]

    barrier = pltpu.get_barrier_semaphore()
    peers = [xr, xl, zr, zl, zo, nxt, prv] + others
    for peer in peers:
        pl.semaphore_signal(barrier, inc=1, device_id=peer, device_id_type=MESH)
    pl.semaphore_wait(barrier, len(peers))

    tok = ChipGather(
        [tokens.at[pl.ds(p * half_rows, half_rows)] for p in (0, 1)], tb, core,
        chip(1, core), chip(ny - 1, core), partner, (t_ysend, t_yrecv, t_fsend, t_psend, t_precv),
    )
    wts = ChipGather(
        [o_window, o_latent], wb, core,
        chip(1, core), chip(ny - 1, core), partner, (w_ysend, w_yrecv, w_fsend, w_psend, w_precv),
    )
    tok.start()
    for p in (0, 1):
        tb[0, core, p] = tokens[p * half_rows : (p + 1) * half_rows]

    mref[...] = jnp.full(mref.shape, NEG, f32)
    lref[...] = jnp.zeros(lref.shape, f32)
    acc[...] = jnp.zeros(acc.shape, f32)
    ssend[...] = jnp.zeros(ssend.shape, f32)
    pacc[...] = jnp.zeros(pacc.shape, f32)
    sq[...] = jnp.zeros(sq.shape, f32)
    for c in loads:
        c.wait()
    wcat[:, 128:256] = jnp.concatenate([wk[...], wv[...]], axis=1)
    wcat[:, 256:384] = jnp.concatenate([wr[...], jnp.zeros((D, 96), bf16)], axis=1)

    @pl.loop(0, 4)
    def _(slot):
        chip_at = (y + ny - (slot + slot // 2 - 2 * (slot // 3))) % ny
        w_rows = pl.ds(pl.multiple_of(chip_at * 512, 512), 512)

        @pl.loop(0, 2)
        def _(part):
            for s in range(4):
                for p in (0, 1):
                    @pl.when((slot == s) & (part == p))
                    def _():
                        if s:
                            tok.arrive(s, p)
                        tok.partner(s, p)
                        if (s, p) == (2, 1):
                            wts.start()
            t32 = jnp.concatenate([tb[slot, 0, part], tb[slot, 1, part]], axis=1).astype(f32)
            out_rows = pl.ds(pl.multiple_of(part * half_rows, half_rows), half_rows)
            squares = t32 * t32
            sq[out_rows] += (
                squares[:, 0:128] + squares[:, 128:256] + squares[:, 256:384] + squares[:, 384:512]
            )
            scaled = (t32 * norm_gain[pl.ds(chip_at, 1), :]).astype(bf16)
            for w, lo, hi in ((wdl, 768, 1280), (wcat, 1280, 1664), (wdq, 0, 768)):
                pacc[out_rows, lo:hi] += jnp.dot(scaled, w[w_rows, :], preferred_element_type=f32)

    cos_f, sin_f = far[0:16, 0:1], far[16:32, 0:1]
    cos_n, sin_n = near[0:16, :], near[16:32, :]
    cos = cos_f * cos_n - sin_f * sin_n
    sin = sin_f * cos_n + cos_f * sin_n
    near[0:16, :] = cos
    near[16:32, :] = sin
    row_scale = lax.rsqrt(jnp.sum(sq[...], axis=1, keepdims=True) * (1.0 / D) + EPS)

    def normed(lo, hi, gain):
        v = (pacc[:, lo:hi] * row_scale).astype(bf16).astype(f32)
        scale = lax.rsqrt(jnp.sum(v * v, axis=1, keepdims=True) * (1.0 / (hi - lo)) + EPS)
        return (v * scale * gain[...]).astype(bf16)

    quarter = rows // 4
    up_kv = jnp.concatenate([uk[...], uv[...]], axis=1)
    kv = jnp.dot(normed(768, 1280, latent_gain), up_kv, preferred_element_type=f32)
    kvm[0:rows] = kv[:, 0:128].astype(bf16)
    for b in range(rows // 128):
        block = kv[128 * b : 128 * b + 128, 128:256].T
        kvm[rows + quarter + 128 * b : rows + quarter + 128 * b + 128] = block.astype(bf16)
    rr = (pacc[:, 1536:1664] * row_scale).astype(bf16).astype(f32).T
    ra, rb = rr[0:16], rr[16:32]
    cos, sin = near[0:16, :], near[16:32, :]
    turned = jnp.concatenate([ra * cos - rb * sin, rb * cos + ra * sin, jnp.zeros((96, rows), f32)], axis=0).T
    packed = turned[0:quarter]
    for g in range(1, 4):
        packed = packed + pltpu.roll(turned[g * quarter : (g + 1) * quarter], 32 * g, 1)
    kvm[rows : rows + quarter] = packed.astype(bf16)
    half = kvm.shape[0] // 2
    k_out = {}
    for order in ((0, 1), (1, 0)):
        for which, h in ((0, order[0]), (1, order[1])):
            slot, dev = ((1, xr), (2, xl))[which]
            k_out[(which, h)] = remote(
                kvm.at[pl.ds(h * half, half)], kvb.at[slot, pl.ds(h * half, half)],
                k_send.at[which, h], k_recv.at[which, h], dev,
            )
    for key in ((0, 0), (1, 1), (0, 1), (1, 0)):
        k_out[key].start()
    kvb[0] = kvm[...]

    qf = jnp.dot(normed(0, 768, query_gain), uq[...], preferred_element_type=f32) * (LOG2E * 96 ** (-0.5))
    for t in range(tiles):
        qq = jnp.concatenate([qf[QT * t : QT * t + QT], jnp.zeros((QT, 64), f32)], axis=1).T
        ct, st = cos[:, QT * t : QT * t + QT], sin[:, QT * t : QT * t + QT]
        for h in range(2):
            a, b = qq[96 * h + 64 : 96 * h + 80], qq[96 * h + 80 : 96 * h + 96]
            qb[0, h, t] = jnp.concatenate(
                [qq[96 * h : 96 * h + 64], a * ct - b * st, b * ct + a * st], axis=0
            ).astype(bf16)
    qt = qb.at[0]
    q_out = {}
    for order in ((0, 1), (1, 0)):
        for which, h in ((0, order[0]), (1, order[1])):
            slot, dev = ((1, zr), (2, zl))[which]
            q_out[(which, h)] = remote(
                qt.at[h], qb.at[slot, h], q_send.at[which, h], q_recv.at[which, h], dev
            )
    for key in ((0, 0), (1, 1), (0, 1), (1, 0)):
        q_out[key].start()

    kvw[...] = (pacc[:, 1408:1536] * row_scale).astype(bf16)
    halo = [
        remote(kvw.at[pl.ds(rows - WINDOW, WINDOW)], kvp.at[pl.ds(0, WINDOW)], h_send.at[0], h_recv.at[0], nxt),
        remote(kvw.at[pl.ds(0, WINDOW)], kvp.at[pl.ds(rows + WINDOW, WINDOW)], h_send.at[1], h_recv.at[1], prv),
    ]
    for c in halo:
        c.start()
    kvp[WINDOW : WINDOW + rows] = kvw[...]
    wq = pacc[:, 1280:1408] * row_scale
    for t in range(tiles):
        qwt[t] = wq[QT * t : QT * t + QT].T.astype(bf16).reshape(2, 64, QT)
    q_fwd = [
        remote(qb.at[1, 0], qb.at[3, 0], qf_send.at[0], qf_recv.at[0], zr),
        remote(qb.at[2, 1], qb.at[3, 1], qf_send.at[1], qf_recv.at[1], zl),
    ]
    k_fwd = [
        remote(kvb.at[1, pl.ds(0, half)], kvb.at[3, pl.ds(0, half)], kf_send.at[0], kf_recv.at[0], xr),
        remote(kvb.at[2, pl.ds(half, half)], kvb.at[3, pl.ds(half, half)], kf_send.at[1], kf_recv.at[1], xl),
    ]

    def unpack(i):
        packed = kvb[i, rows : rows + quarter].astype(f32)
        for g in range(4):
            moved = packed if g == 0 else pltpu.roll(packed, 128 - 32 * g, 1)
            rotx[i, g * quarter : (g + 1) * quarter] = moved.astype(bf16)

    def piece(part, src, d, cc):
        dev = chip(d, cc) if d else partner
        slot = (0, 1, 3, 2)[d]
        row_at = pl.ds(pl.multiple_of(dev[1] * mine, mine), mine)
        i = 2 * d + (cc if d else 0)
        return remote(
            src.at[row_at], orow.at[slot, core, part], a_send.at[part, i], a_recv.at[part, slot, core], dev
        )

    def pieces(part, src):
        keys = [(2, 0), (2, 1), (1, 0), (3, 0), (1, 1), (3, 1), (0, 0)]
        return [piece(part, src, d, cc) for d, cc in keys]

    S = ((s00, s01), (s10, s11))
    X = ((x00, x01), (x10, x11))

    def stage_a(k, q, t, slot):
        z64, z96 = jnp.zeros((64, QT), bf16), jnp.zeros((96, QT), bf16)
        keys = jnp.concatenate([kvb[k, 0:rows], rotx[k]], axis=1)
        for h in range(2):
            qq = qb[q, h, t]
            if h == 0:
                parts = [qq[0:64], z64, qq[64:96], z96]
            else:
                parts = [z64, qq[0:64], qq[64:96], z96]
            s = jnp.dot(keys, jnp.concatenate(parts, axis=0), preferred_element_type=f32)
            S[slot][h][...] = s
            X[slot][h][...] = jnp.max(s.reshape(rows // 8, 8, QT), axis=0)

    def stage_b(k, q, t, slot):
        for h in range(2):
            old = mref[q, t, h : h + 1]
            new = jnp.maximum(old, jnp.max(X[slot][h][...], axis=0, keepdims=True))
            alpha = jnp.exp2(old - new)
            mref[q, t, h : h + 1] = new
            total = None
            for c in range(rows // 256):
                p = jnp.exp2(S[slot][h][c * 256 : (c + 1) * 256] - new).astype(bf16)
                base = rows + quarter + 256 * c + 64 * h
                v = jnp.concatenate([kvb[k, base : base + 64], kvb[k, base + 128 : base + 192]], axis=1)
                v = jnp.concatenate([v, jnp.ones((16, 256), bf16)], axis=0)
                o = jnp.dot(v, p, preferred_element_type=f32)
                total = o if total is None else total + o
            lref[q, t, h : h + 1] = lref[q, t, h : h + 1] * alpha + total[64:65]
            acc[q, t, 64 * h : 64 * h + 64] = acc[q, t, 64 * h : 64 * h + 64] * alpha + total[0:64]

    def pipeline(n, where, before=None):
        def A(i, slot):
            stage_a(*where(i), slot)

        def B(i, slot):
            stage_b(*where(i), slot)

        A(0, 0)
        loops = (n - 1) // 2

        @pl.loop(0, loops)
        def _(j):
            i = 2 * j
            if before is not None:
                before(i + 1)
            A(i + 1, 1)
            B(i, 0)
            if before is not None:
                before(i + 2)
            A(i + 2, 0)
            B(i + 1, 1)

        i = 2 * loops
        if n % 2 == 0:
            if before is not None:
                before(i + 1)
            A(i + 1, 1)
            B(i, 0)
            B(i + 1, 1)
        else:
            B(i, 0)

    def window():
        for c in halo:
            c.wait_recv()
        span = QT + 2 * WINDOW
        key_i = lax.broadcasted_iota(jnp.int32, (span, QT), 0)
        dist = key_i - WINDOW - lax.broadcasted_iota(jnp.int32, (span, QT), 1)
        dist = jnp.abs(dist)
        distf = dist.astype(f32)

        @pl.loop(0, tiles)
        def _(t):
            rows_at = pl.ds(pl.multiple_of(t * QT, QT), span)
            kv = kvp[rows_at]
            pos = sp * rows + t * QT + key_i - WINDOW
            valid = (dist <= WINDOW) & (pos >= 0) & (pos < nsp * rows)
            for h in range(2):
                slope, sink = slopes[tp * 2 + h], sinks[h]
                rhs = jnp.concatenate([qwt[t, h], jnp.zeros((64, QT), bf16)], axis=0)
                s = jnp.dot(kv, rhs, preferred_element_type=f32) * 0.125
                s = jnp.where(valid, s - slope * distf, NEG)
                m = jnp.maximum(jnp.max(s, axis=0, keepdims=True), sink)
                w = jnp.exp2((s - m) * LOG2E)
                denom = jnp.sum(w, axis=0, keepdims=True) + jnp.exp2((sink - m) * LOG2E)
                w = (w * (1.0 / denom)).astype(bf16)
                o = lax.dot_general(kv, w, (((0,), (0,)), ((), ())), preferred_element_type=f32)
                S[0][0][h * 64 : h * 64 + 64] = o[64:128]
            osw[pl.ds(pl.multiple_of(t * QT, QT), QT), :] = S[0][0][0:128].T.astype(bf16)

    unpack(0)

    @pl.loop(0, 3)
    def _(q):
        @pl.when(q == 1)
        def _():
            window()
            for c in pieces(0, osw):
                c.start()
            orow[0, core, 0] = osw[pl.ds(pl.multiple_of(tp * mine, mine), mine), :]
            for c, f in ((q_out[(0, 0)], q_fwd[0]), (q_out[(1, 1)], q_fwd[1])):
                c.wait_recv()
                f.start()
            q_out[(0, 1)].wait_recv()

        @pl.when(q == 2)
        def _():
            q_out[(1, 0)].wait_recv()
            for c, f in ((k_out[(0, 0)], k_fwd[0]), (k_out[(1, 1)], k_fwd[1])):
                c.wait_recv()
                f.start()

        pipeline(tiles, lambda i: (0, q, i))

    k_out[(0, 1)].wait_recv()
    k_out[(1, 0)].wait_recv()
    unpack(1)
    unpack(2)
    for c in q_fwd:
        c.wait_recv()

    def arrive(i):
        @pl.when(i == 3 * tiles)
        def _():
            for c in k_fwd:
                c.wait_recv()
            unpack(3)

    def finish(q):
        for t in range(tiles):
            for h in range(2):
                inv = 1.0 / lref[q, t, h : h + 1]
                osend[q, t, 64 * h : 64 * h + 64] = (acc[q, t, 64 * h : 64 * h + 64] * inv).astype(bf16)
            ssend[q, t, 0:2] = mref[q, t, 0:2]
            ssend[q, t, 2:4] = lref[q, t, 0:2]

    back = {}
    for q, slot, dev in ((3, 3, zo), (2, 1, zr), (1, 2, zl)):
        back[q] = (
            remote(osend.at[q], obuf.at[slot], o_send.at[q], o_recv.at[slot], dev),
            remote(ssend.at[q], sbuf.at[slot], s_send.at[q], s_recv.at[slot], dev),
        )

    pipeline(4 * tiles, lambda i: (i // tiles, 3, i % tiles), arrive)
    finish(3)
    for c in back[3]:
        c.start()
    wts.arrive(1, 0)
    wts.arrive(2, 1)

    @pl.loop(0, 3)
    def _(r):
        q = 2 - r
        pipeline(3 * tiles, lambda i: (1 + i // tiles, q, i % tiles))
        finish(q)
        for n in (0, 1):
            @pl.when(r == n)
            def _():
                for c in back[2 - n]:
                    c.start()
                if n == 1:
                    wts.arrive(1, 1)
                    wts.arrive(2, 0)

    for q in (3, 2, 1):
        for c in back[q]:
            c.wait_recv()

    @pl.loop(0, tiles)
    def _(t):
        ms = [ssend[0, t, 0:2]] + [sbuf[j, t, 0:2] for j in (1, 2, 3)]
        ls = [ssend[0, t, 2:4]] + [sbuf[j, t, 2:4] for j in (1, 2, 3)]
        top = jnp.maximum(jnp.maximum(ms[0], ms[1]), jnp.maximum(ms[2], ms[3]))
        ws = [l * jnp.exp2(m - top) for m, l in zip(ms, ls)]
        inv = 1.0 / (ws[0] + ws[1] + ws[2] + ws[3])
        for h in range(2):
            rows_h = slice(64 * h, 64 * h + 64)
            total = osend[0, t, rows_h].astype(f32) * (ws[0] * inv)[h : h + 1]
            for j in (1, 2, 3):
                total = total + obuf[j, t, rows_h].astype(f32) * (ws[j] * inv)[h : h + 1]
            S[0][0][rows_h] = total
        osl[pl.ds(pl.multiple_of(t * QT, QT), QT), :] = S[0][0][0:128].T.astype(bf16)

    for c in pieces(1, osl):
        c.start()
    orow[0, core, 1] = osl[pl.ds(pl.multiple_of(tp * mine, mine), mine), :]
    wts.arrive(3, 0)
    wts.arrive(3, 1)
    for s in range(4):
        for p in (0, 1):
            wts.partner(s, p)
            for cc in (0, 1) if s else (1 - core,):
                there = orow.at[s, cc, p]
                remote(there, there, a_send.at[p, 0], a_recv.at[p, s, cc], partner).wait_recv()

    @pl.loop(0, D // 512)
    def _(b):
        cols = pl.ds(pl.multiple_of(b * 512, 512), 512)
        total = None
        for s in range(4):
            for cc in (0, 1):
                o = jnp.concatenate([orow[s, cc, 0], orow[s, cc, 1]], axis=1)
                w = jnp.concatenate([wb[s, cc, 0, :, cols], wb[s, cc, 1, :, cols]], axis=0)
                g = jnp.dot(o, w, preferred_element_type=f32).astype(bf16).astype(f32)
                total = g if total is None else total + g
        result[:, cols] = total.astype(bf16)

    for c in halo + list(q_out.values()) + list(k_out.values()) + q_fwd + k_fwd:
        c.wait_send()
    for q in (3, 2, 1):
        for c in back[q]:
            c.wait_send()
    for part, src in ((0, osw), (1, osl)):
        for c in pieces(part, src):
            c.wait_send()
    tok.drain()
    wts.drain()


def angle_tables(rows, nsp):
    inverse = THETA ** (-np.arange(16, dtype=np.float64) / 16)
    far = np.arange(nsp)[:, None] * rows * inverse[None, :]
    far = np.concatenate([np.cos(far), np.sin(far)], axis=1)[:, :, None]
    near = inverse[:, None] * np.arange(rows)[None, :]
    near = np.concatenate([np.cos(near), np.sin(near)], axis=0)
    return np.broadcast_to(far, (nsp, 32, 128)).astype(np.float32), near.astype(np.float32)


def per_device(
    nsp, ntp, tokens, norm_gain, window_query, window_key, window_value, sink_logit, down_query,
    down_latent, rotary_proj, query_gain, latent_gain, up_query, up_key, up_value, window_out, latent_out,
):
    rows = tokens.shape[0]
    tiles, mine, half_rows = rows // QT, rows // ntp, rows // 2
    far, near = angle_tables(rows, nsp)
    slopes = np.exp2(-8.0 * (np.arange(A_HEADS) + 1.0) / A_HEADS).astype(np.float32)
    dma, V = pltpu.SemaphoreType.DMA, pltpu.VMEM
    vm, smem = pl.BlockSpec(memory_space=pltpu.VMEM), pl.BlockSpec(memory_space=pltpu.SMEM)
    hbm = pl.BlockSpec(memory_space=pl.ANY)
    gather_sems = [dma((3, 2)), dma((4, 2)), dma((2,)), dma((4, 2)), dma((4, 2))]
    message = rows + rows // 4 + rows
    return pl.pallas_call(
        functools.partial(layer_kernel, rows, nsp // NX, NX, ntp // 2),
        out_shape=jax.ShapeDtypeStruct((mine, D), bf16),
        in_specs=[vm, vm, vm, vm, smem, smem] + [hbm] * 13,
        out_specs=vm,
        scratch_shapes=[
            V((4, 2, 2, half_rows, 256), bf16), V((4, 2, 2, 128, D), bf16),
            V((D, 768), bf16), V((D, 512), bf16), V((D, 384), bf16),
            V((D, 64), bf16), V((D, 64), bf16), V((D, 32), bf16),
            V((768, 192), bf16), V((512, 128), bf16), V((512, 128), bf16),
            V((32, 128), f32), V((32, rows), f32), V((rows, 1664), f32), V((rows, 128), f32),
            V((message, 128), bf16), V((tiles, 2, 64, QT), bf16), V((rows, 128), bf16),
            V((rows, 128), bf16), V((rows, 128), bf16), V((4, 2, 2, mine, 128), bf16),
            V((4, message, 128), bf16), V((4, rows, 128), bf16), V((4, 2, tiles, 96, QT), bf16),
            V((rows + 2 * WINDOW, 128), bf16),
            V((4, tiles, 8, QT), f32), V((4, tiles, 8, QT), f32), V((4, tiles, 128, QT), f32),
        ]
        + [V((rows, QT), f32)] * 4 + [V((8, QT), f32)] * 4
        + [
            V((4, tiles, 128, QT), bf16), V((4, tiles, 8, QT), f32),
            V((4, tiles, 128, QT), bf16), V((4, tiles, 8, QT), f32),
            dma((13,)),
        ]
        + gather_sems + gather_sems
        + [
            dma((2, 8)), dma((2, 4, 2)),
            dma((2,)), dma((2,)), dma((2, 2)), dma((2, 2)), dma((2,)), dma((2,)),
            dma((2, 2)), dma((2, 2)), dma((2,)), dma((2,)),
            dma((4,)), dma((4,)), dma((4,)), dma((4,)),
        ],
        compiler_params=pltpu.CompilerParams(
            collective_id=1, has_side_effects=True, vmem_limit_bytes=60 * 2**20
        ),
        name="layer",
    )(
        tokens, norm_gain.reshape(4, D // 4), query_gain.reshape(1, -1), latent_gain.reshape(1, -1),
        sink_logit, jnp.asarray(slopes), window_query, window_key, window_value, down_query, down_latent,
        rotary_proj, up_query, up_key, up_value, window_out, latent_out, jnp.asarray(far), jnp.asarray(near),
    )


def solution(mesh):
    col, row, rep = P(None, "tp"), P("tp", None), P()
    placed = (
        P("sp", "tp"), rep, col, col, col, P("tp"), rep, rep, rep, rep, rep, col, col, col, row, row,
    )
    body = functools.partial(per_device, mesh.shape["sp"], mesh.shape["tp"])
    return jax.shard_map(
        body, mesh=mesh, in_specs=placed, out_specs=P(("sp", "tp"), None), check_vma=False
    )
```

time: 157 us -> 98.3 us (0.63); the launches traced: 154 us -> 97.9 us
  waiting for transfers between devices: 70.1 us -> 0 us
  Pallas kernels: 37.5 us -> 85.9 us
  matrix products: 20.1 us -> 0 us
  between operations: 13.8 us -> 0.01 us
  other arithmetic: 5.99 us -> 0 us
  local copies, waits for them, and re-layouts: 6.86 us -> 12.1 us
    pallas_call x1, Pallas kernels: 37.5 us -> 85.9 us  [per_device(): pl.pallas_call(functools.partial(layer_kernel, rows, nsp // NX, NX, ntp /...]
    all_gather x1 -> x0, waiting for transfers between devices: 35.6 us -> none  [per_device(): as_float = lax.all_gather(tokens, 'tp', axis=1, tiled=True).astype(f32)]
    reduce_scatter x1 -> x0, waiting for transfers between devices: 33.7 us -> none  [per_device(): return lax.psum_scatter(part, 'tp', scatter_dimension=0, tiled=True)]
    dot_general x10 -> x0, matrix products: 20.1 us -> none  [the longest x6 15.1 us: project(): jnp.dot(scaled, weight, preferred_element_type=f32) * row_scale]
    unnamed x44 -> x5, local copies, waits for them, and re-layouts: 3.82 us -> 9.49 us
    reduce_sum x1 -> x0, other arithmetic: 2.72 us -> none  [per_device(): jnp.sum(as_float * as_float, axis=1) / width + EPS]
    another operation x2 -> x0, other arithmetic: 1.94 us -> none
  transfers between devices with their start and end apart: 2 -> 0, of which waited for: 2 -> 0; matrix products, arithmetic and copies ran while one was open for 1% -> 0% of each run, Pallas kernels for 0% -> 0%
where the time goes in v2:
time: 98.3 us; the launch traced here: 97.9 us
  Pallas kernels  85.9 us (87%)
  local copies, waits for them, and re-layouts  12.1 us (12%)
    pallas_call x1, Pallas kernels, per_device(): pl.pallas_call(functools.partial(layer_kernel, rows, nsp // NX, NX, ntp /...  85.9 us
    unnamed x5, local copies, waits for them, and re-layouts  9.49 us

profile of v2, /device:TPU:1, one launch (start us, length us, event | category | flops | bytes accessed | tf_op | source)
XLA Modules:
  0.0 97.9 jit_solution(10550598501353192743)
XLA Ops:
  0.0 1.3 %reshape.10.query_gain = f32[1,768]{1,0:T(1,128)} reshape(f32[768]{0:T(1024)} %param.28) | data formatting | bytes 6144 | tf_op jit(solution)/shard_map/reshape | solution.py:556
  1.3 1.3 %reshape.9.norm_gain = f32[4,512]{1,0:T(4,128)} reshape(f32[2048]{0:T(1024)} %param.20) | data formatting | bytes 16384 | tf_op jit(solution)/shard_map/reshape | solution.py:556
  2.6 1.9 %copy.23.u_query = bf16[768,192]{1,0:T(8,128)(2,1)} copy(bf16[768,192]{0,1:T(8,128)(2,1)} %param.30) | data formatting | bytes 589824 | tf_op args[11]
  4.4 1.9 %copy.20.w_key = bf16[2048,64]{1,0:T(8,128)(2,1)} copy(bf16[2048,64]{0,1:T(8,128)(2,1)} %param.22) | data formatting | bytes 524288 | tf_op args[3]
  6.4 2.0 %copy.21.w_value = bf16[2048,64]{1,0:T(8,128)(2,1)} copy(bf16[2048,64]{0,1:T(8,128)(2,1)} %param.23) | data formatting | bytes 524288 | tf_op args[4]
  8.4 1.9 %copy.22.w_rot = bf16[2048,32]{1,0:T(8,128)(2,1)} copy(bf16[2048,32]{0,1:T(8,128)(2,1)} %param.27) | data formatting | bytes 262144 | tf_op args[8]
  10.3 85.9 %layer.1 = bf16[96,2048]{1,0:T(8,128)(2,1)} custom-call(bf16[768,256]{1,0:T(8,128)(2,1)} %tokens.1, f32[4,512]{1,0:T(4,128)} %reshape.9.norm_gain, f32[1,768]{1,0:T(1,128)} %reshape.10.query_gain, f32[1,512]{1,0:T(1,128)} %bitcast.1, f32[2]{0:T(128)} %sinks.1, f32[16]{0:T(128)} %constant.6.clone.slopes, bf16[2048,128]{1,0:T(8,128)(2,1)} %w_query.1, ...), custom_call_target="tpu_custom_call" | custom-call | tf_op jit(solution)/shard_map/layer/pallas_call | solution.py:521
  96.2 1.8 %copy.25 = bf16[96,2048]{1,0:T(8,128)(2,1)} copy(bf16[96,2048]{1,0:T(8,128)(2,1)} %layer.1) | data formatting | bytes 786432

commit v3 on v2

--- a/solution.py
+++ b/solution.py
@@ -77,7 +77,7 @@
     w_query, w_key, w_value, d_query, d_latent, w_rot, u_query, u_key, u_value, o_window, o_latent,
     tab_far, tab_near,
     result,
-    tb, wb, wdq, wdl, wcat, wk, wv, wr, uq, uk, uv, far, near, pacc, sq,
+    tb, wb, wdq, wdl, wcat, wnarrow, uq, uk, uv, far, near, pacc, sq,
     kvm, qwt, kvw, osw, osl, orow,
     kvb, rotx, qb, kvp, mref, lref, acc, s00, s01, s10, s11, x00, x01, x10, x11,
     osend, ssend, obuf, sbuf,
@@ -98,8 +98,9 @@
     loads = [
         pltpu.make_async_copy(s, d, l_sem.at[i])
         for i, (s, d) in enumerate((
-            (d_query, wdq), (d_latent, wdl), (w_query, wcat.at[:, pl.ds(0, 128)]), (w_key, wk),
-            (w_value, wv), (w_rot, wr), (u_query, uq), (u_key, uk), (u_value, uv),
+            (d_query, wdq), (d_latent, wdl), (w_query, wcat.at[:, pl.ds(0, 128)]),
+            (w_key, wnarrow.at[pl.ds(0, 64)]), (w_value, wnarrow.at[pl.ds(64, 64)]),
+            (w_rot, wnarrow.at[pl.ds(128, 32)]), (u_query, uq), (u_key, uk), (u_value, uv),
             (tab_far.at[sp], far), (tab_near, near),
             (o_window, wb.at[0, core, 0]), (o_latent, wb.at[0, core, 1]),
         ))
@@ -143,10 +144,16 @@
     ssend[...] = jnp.zeros(ssend.shape, f32)
     pacc[...] = jnp.zeros(pacc.shape, f32)
     sq[...] = jnp.zeros(sq.shape, f32)
+    wnarrow[160:256] = jnp.zeros((96, D), bf16)
     for c in loads:
         c.wait()
-    wcat[:, 128:256] = jnp.concatenate([wk[...], wv[...]], axis=1)
-    wcat[:, 256:384] = jnp.concatenate([wr[...], jnp.zeros((D, 96), bf16)], axis=1)
+
+    @pl.loop(0, D // 128)
+    def _(b):
+        at_b = pl.ds(pl.multiple_of(b * 128, 128), 128)
+        wcat[at_b, 128:384] = wnarrow[:, at_b].astype(f32).T.astype(bf16)
+
+    arrivals = {(1, 0): ((1, 0), (2, 1)), (1, 1): ((1, 1), (2, 0)), (3, 0): ((3, 0), (3, 1))}
 
     @pl.loop(0, 4)
     def _(slot):
@@ -159,18 +166,16 @@
                 for p in (0, 1):
                     @pl.when((slot == s) & (part == p))
                     def _():
-                        if s:
-                            tok.arrive(s, p)
+                        for key in arrivals.get((s, p), ()):
+                            tok.arrive(*key)
                         tok.partner(s, p)
-                        if (s, p) == (2, 1):
-                            wts.start()
             t32 = jnp.concatenate([tb[slot, 0, part], tb[slot, 1, part]], axis=1).astype(f32)
             out_rows = pl.ds(pl.multiple_of(part * half_rows, half_rows), half_rows)
             squares = t32 * t32
             sq[out_rows] += (
                 squares[:, 0:128] + squares[:, 128:256] + squares[:, 256:384] + squares[:, 384:512]
             )
-            scaled = (t32 * norm_gain[pl.ds(chip_at, 1), :]).astype(bf16)
+            scaled = (t32 * norm_gain[:, w_rows]).astype(bf16)
             for w, lo, hi in ((wdl, 768, 1280), (wcat, 1280, 1664), (wdq, 0, 768)):
                 pacc[out_rows, lo:hi] += jnp.dot(scaled, w[w_rows, :], preferred_element_type=f32)
 
@@ -185,11 +190,18 @@
     def normed(lo, hi, gain):
         v = (pacc[:, lo:hi] * row_scale).astype(bf16).astype(f32)
         scale = lax.rsqrt(jnp.sum(v * v, axis=1, keepdims=True) * (1.0 / (hi - lo)) + EPS)
-        return (v * scale * gain[...]).astype(bf16)
-
+        return (v * scale * gain).astype(bf16)
+
+    kvw[...] = (pacc[:, 1408:1536] * row_scale).astype(bf16)
+    halo = [
+        remote(kvw.at[pl.ds(rows - WINDOW, WINDOW)], kvp.at[pl.ds(0, WINDOW)], h_send.at[0], h_recv.at[0], nxt),
+        remote(kvw.at[pl.ds(0, WINDOW)], kvp.at[pl.ds(rows + WINDOW, WINDOW)], h_send.at[1], h_recv.at[1], prv),
+    ]
+    for c in halo:
+        c.start()
     quarter = rows // 4
     up_kv = jnp.concatenate([uk[...], uv[...]], axis=1)
-    kv = jnp.dot(normed(768, 1280, latent_gain), up_kv, preferred_element_type=f32)
+    kv = jnp.dot(normed(768, 1280, latent_gain[...]), up_kv, preferred_element_type=f32)
     kvm[0:rows] = kv[:, 0:128].astype(bf16)
     for b in range(rows // 128):
         block = kv[128 * b : 128 * b + 128, 128:256].T
@@ -215,15 +227,16 @@
         k_out[key].start()
     kvb[0] = kvm[...]
 
-    qf = jnp.dot(normed(0, 768, query_gain), uq[...], preferred_element_type=f32) * (LOG2E * 96 ** (-0.5))
-    for t in range(tiles):
-        qq = jnp.concatenate([qf[QT * t : QT * t + QT], jnp.zeros((QT, 64), f32)], axis=1).T
-        ct, st = cos[:, QT * t : QT * t + QT], sin[:, QT * t : QT * t + QT]
-        for h in range(2):
-            a, b = qq[96 * h + 64 : 96 * h + 80], qq[96 * h + 80 : 96 * h + 96]
-            qb[0, h, t] = jnp.concatenate(
-                [qq[96 * h : 96 * h + 64], a * ct - b * st, b * ct + a * st], axis=0
-            ).astype(bf16)
+    qf = lax.dot_general(
+        uq[...], normed(0, 768, jnp.concatenate([query_gain[i : i + 1] for i in range(6)], axis=1)), (((1,), (1,)), ((), ())), preferred_element_type=f32
+    ) * (LOG2E * 96 ** (-0.5))
+    for h in range(2):
+        a, b = qf[96 * h + 64 : 96 * h + 80], qf[96 * h + 80 : 96 * h + 96]
+        whole = jnp.concatenate(
+            [qf[96 * h : 96 * h + 64], a * cos - b * sin, b * cos + a * sin], axis=0
+        ).astype(bf16)
+        for t in range(tiles):
+            qb[0, h, t] = whole[:, QT * t : QT * t + QT]
     qt = qb.at[0]
     q_out = {}
     for order in ((0, 1), (1, 0)):
@@ -235,13 +248,7 @@
     for key in ((0, 0), (1, 1), (0, 1), (1, 0)):
         q_out[key].start()
 
-    kvw[...] = (pacc[:, 1408:1536] * row_scale).astype(bf16)
-    halo = [
-        remote(kvw.at[pl.ds(rows - WINDOW, WINDOW)], kvp.at[pl.ds(0, WINDOW)], h_send.at[0], h_recv.at[0], nxt),
-        remote(kvw.at[pl.ds(0, WINDOW)], kvp.at[pl.ds(rows + WINDOW, WINDOW)], h_send.at[1], h_recv.at[1], prv),
-    ]
-    for c in halo:
-        c.start()
+    wts.start()
     kvp[WINDOW : WINDOW + rows] = kvw[...]
     wq = pacc[:, 1280:1408] * row_scale
     for t in range(tiles):
@@ -307,12 +314,14 @@
             lref[q, t, h : h + 1] = lref[q, t, h : h + 1] * alpha + total[64:65]
             acc[q, t, 64 * h : 64 * h + 64] = acc[q, t, 64 * h : 64 * h + 64] * alpha + total[0:64]
 
-    def pipeline(n, where, before=None):
+    def pipeline(n, where, before=None, after=None):
         def A(i, slot):
             stage_a(*where(i), slot)
 
         def B(i, slot):
             stage_b(*where(i), slot)
+            if after is not None:
+                after(i)
 
         A(0, 0)
         loops = (n - 1) // 2
@@ -405,45 +414,54 @@
                 c.wait_recv()
             unpack(3)
 
-    def finish(q):
-        for t in range(tiles):
-            for h in range(2):
-                inv = 1.0 / lref[q, t, h : h + 1]
-                osend[q, t, 64 * h : 64 * h + 64] = (acc[q, t, 64 * h : 64 * h + 64] * inv).astype(bf16)
-            ssend[q, t, 0:2] = mref[q, t, 0:2]
-            ssend[q, t, 2:4] = lref[q, t, 0:2]
-
-    back = {}
-    for q, slot, dev in ((3, 3, zo), (2, 1, zr), (1, 2, zl)):
-        back[q] = (
-            remote(osend.at[q], obuf.at[slot], o_send.at[q], o_recv.at[slot], dev),
-            remote(ssend.at[q], sbuf.at[slot], s_send.at[q], s_recv.at[slot], dev),
+    def finish(q, t):
+        for h in range(2):
+            inv = 1.0 / lref[q, t, h : h + 1]
+            osend[q, t, 64 * h : 64 * h + 64] = (acc[q, t, 64 * h : 64 * h + 64] * inv).astype(bf16)
+        ssend[q, t, 0:2] = mref[q, t, 0:2]
+        ssend[q, t, 2:4] = lref[q, t, 0:2]
+
+    def back(q, t):
+        slot, dev = {3: (3, zo), 2: (1, zr), 1: (2, zl)}[q]
+        return (
+            remote(osend.at[q, t], obuf.at[slot, t], o_send.at[q, t], o_recv.at[slot, t], dev),
+            remote(ssend.at[q, t], sbuf.at[slot, t], s_send.at[q, t], s_recv.at[slot, t], dev),
         )
 
     pipeline(4 * tiles, lambda i: (i // tiles, 3, i % tiles), arrive)
-    finish(3)
-    for c in back[3]:
-        c.start()
+    for t in range(tiles):
+        finish(3, t)
+    for t in range(tiles):
+        for c in back(3, t):
+            c.start()
     wts.arrive(1, 0)
     wts.arrive(2, 1)
 
     @pl.loop(0, 3)
     def _(r):
         q = 2 - r
-        pipeline(3 * tiles, lambda i: (1 + i // tiles, q, i % tiles))
-        finish(q)
-        for n in (0, 1):
-            @pl.when(r == n)
+
+        def done(i):
+            @pl.when(i % 3 == 2)
             def _():
-                for c in back[2 - n]:
-                    c.start()
-                if n == 1:
-                    wts.arrive(1, 1)
-                    wts.arrive(2, 0)
+                finish(q, i // 3)
+                for n in (0, 1):
+                    @pl.when(r == n)
+                    def _():
+                        for c in back(2 - n, i // 3):
+                            c.start()
+
+        pipeline(3 * tiles, lambda i: (1 + i % 3, q, i // 3), after=done)
+
+        @pl.when(r == 1)
+        def _():
+            wts.arrive(1, 1)
+            wts.arrive(2, 0)
 
     for q in (3, 2, 1):
-        for c in back[q]:
-            c.wait_recv()
+        for t in range(tiles):
+            for c in back(q, t):
+                c.wait_recv()
 
     @pl.loop(0, tiles)
     def _(t):
@@ -487,8 +505,9 @@
     for c in halo + list(q_out.values()) + list(k_out.values()) + q_fwd + k_fwd:
         c.wait_send()
     for q in (3, 2, 1):
-        for c in back[q]:
-            c.wait_send()
+        for t in range(tiles):
+            for c in back(q, t):
+                c.wait_send()
     for part, src in ((0, osw), (1, osl)):
         for c in pieces(part, src):
             c.wait_send()
@@ -526,8 +545,8 @@
         scratch_shapes=[
             V((4, 2, 2, half_rows, 256), bf16), V((4, 2, 2, 128, D), bf16),
             V((D, 768), bf16), V((D, 512), bf16), V((D, 384), bf16),
-            V((D, 64), bf16), V((D, 64), bf16), V((D, 32), bf16),
-            V((768, 192), bf16), V((512, 128), bf16), V((512, 128), bf16),
+            V((256, D), bf16),
+            V((192, 768), bf16), V((512, 128), bf16), V((512, 128), bf16),
             V((32, 128), f32), V((32, rows), f32), V((rows, 1664), f32), V((rows, 128), f32),
             V((message, 128), bf16), V((tiles, 2, 64, QT), bf16), V((rows, 128), bf16),
             V((rows, 128), bf16), V((rows, 128), bf16), V((4, 2, 2, mine, 128), bf16),
@@ -546,16 +565,16 @@
             dma((2, 8)), dma((2, 4, 2)),
             dma((2,)), dma((2,)), dma((2, 2)), dma((2, 2)), dma((2,)), dma((2,)),
             dma((2, 2)), dma((2, 2)), dma((2,)), dma((2,)),
-            dma((4,)), dma((4,)), dma((4,)), dma((4,)),
+            dma((4, tiles)), dma((4, tiles)), dma((4, tiles)), dma((4, tiles)),
         ],
         compiler_params=pltpu.CompilerParams(
             collective_id=1, has_side_effects=True, vmem_limit_bytes=60 * 2**20
         ),
         name="layer",
     )(
-        tokens, norm_gain.reshape(4, D // 4), query_gain.reshape(1, -1), latent_gain.reshape(1, -1),
-        sink_logit, jnp.asarray(slopes), window_query, window_key, window_value, down_query, down_latent,
-        rotary_proj, up_query, up_key, up_value, window_out, latent_out, jnp.asarray(far), jnp.asarray(near),
+        tokens, norm_gain.reshape(1, D), query_gain.reshape(6, 128), latent_gain.reshape(1, -1),
+        sink_logit, jnp.asarray(slopes), window_query, window_key.T, window_value.T, down_query, down_latent,
+        rotary_proj.T, up_query.T, up_key, up_value, window_out, latent_out, jnp.asarray(far), jnp.asarray(near),
     )
 
 

time: 98.3 us -> 77.4 us (0.79)
  Pallas kernels: 85.9 us -> 75.5 us
  local copies, waits for them, and re-layouts: 12.1 us -> 1.77 us
    pallas_call x1, Pallas kernels: 85.9 us -> 75.5 us  [per_device(): pl.pallas_call(functools.partial(layer_kernel, rows, nsp // NX, NX, ntp /...]
    unnamed x5 -> x1, local copies, waits for them, and re-layouts: 9.49 us -> 1.77 us
    reshape x2 -> x0, local copies, waits for them, and re-layouts: 2.56 us -> none  [the longest x1 1.29 us: per_device(): norm_gain.reshape(4, D // 4)]
where the time goes in v3:
time: 77.4 us; the launch traced here: 77.2 us
  Pallas kernels  75.5 us (98%)
  local copies, waits for them, and re-layouts  1.77 us (2%)
    pallas_call x1, Pallas kernels, per_device(): pl.pallas_call(functools.partial(layer_kernel, rows, nsp // NX, NX, ntp /...  75.5 us
    unnamed x1, local copies, waits for them, and re-layouts  1.77 us

profile of v3, /device:TPU:1, one launch (start us, length us, event | category | flops | bytes accessed | tf_op | source)
XLA Modules:
  0.0 77.2 jit_solution(7093958014450823963)
XLA Ops:
  0.0 75.5 %layer.1 = bf16[96,2048]{1,0:T(8,128)(2,1)} custom-call(bf16[768,256]{1,0:T(8,128)(2,1)} %tokens.1, f32[1,2048]{1,0:T(1,128)} %bitcast.11, f32[6,128]{1,0:T(8,128)} %bitcast.12, f32[1,512]{1,0:T(1,128)} %bitcast.13, f32[2]{0:T(128)} %sinks.1, f32[16]{0:T(128)} %constant.6.clone.slopes, bf16[2048,128]{1,0:T(8,128)(2,1)} %w_query.1, bf16[64,2048]{1,0:T(8,128)(2,1)} %bitcast.8, ...), custom_call_target="tpu_custom_call" | custom-call | tf_op jit(solution)/shard_map/layer/pallas_call | solution.py:540
  75.5 1.8 %copy.21 = bf16[96,2048]{1,0:T(8,128)(2,1)} copy(bf16[96,2048]{1,0:T(8,128)(2,1)} %layer.1) | data formatting | bytes 786432

commit v4 on v3

--- a/solution.py
+++ b/solution.py
@@ -18,6 +18,7 @@
 QT = 256
 NEG = -1e30
 NX = 4
+PV = 768
 
 
 def remote(src, dst, ss, rs, dev):
@@ -79,7 +80,8 @@
     result,
     tb, wb, wdq, wdl, wcat, wnarrow, uq, uk, uv, far, near, pacc, sq,
     kvm, qwt, kvw, osw, osl, orow,
-    kvb, rotx, qb, kvp, mref, lref, acc, s00, s01, s10, s11, x00, x01, x10, x11,
+    kvb, rotx, qb, kvp, mref, lref, acc,
+    s00, s01, s10, s11, s20, s21, s30, s31, x00, x01, x10, x11, x20, x21, x30, x31, facc,
     osend, ssend, obuf, sbuf,
     l_sem, t_ysend, t_yrecv, t_fsend, t_psend, t_precv, w_ysend, w_yrecv, w_fsend, w_psend, w_precv,
     a_send, a_recv,
@@ -168,6 +170,8 @@
                     def _():
                         for key in arrivals.get((s, p), ()):
                             tok.arrive(*key)
+                        if (s, p) == (1, 1):
+                            wts.start()
                         tok.partner(s, p)
             t32 = jnp.concatenate([tb[slot, 0, part], tb[slot, 1, part]], axis=1).astype(f32)
             out_rows = pl.ds(pl.multiple_of(part * half_rows, half_rows), half_rows)
@@ -236,27 +240,24 @@
             [qf[96 * h : 96 * h + 64], a * cos - b * sin, b * cos + a * sin], axis=0
         ).astype(bf16)
         for t in range(tiles):
-            qb[0, h, t] = whole[:, QT * t : QT * t + QT]
-    qt = qb.at[0]
-    q_out = {}
-    for order in ((0, 1), (1, 0)):
-        for which, h in ((0, order[0]), (1, order[1])):
-            slot, dev = ((1, zr), (2, zl))[which]
-            q_out[(which, h)] = remote(
-                qt.at[h], qb.at[slot, h], q_send.at[which, h], q_recv.at[which, h], dev
-            )
-    for key in ((0, 0), (1, 1), (0, 1), (1, 0)):
-        q_out[key].start()
-
-    wts.start()
+            qb[0, t, h] = whole[:, QT * t : QT * t + QT]
+    q_out = {
+        (slot, t): remote(qb.at[0, t], qb.at[slot, t], q_send.at[slot, t], q_recv.at[slot, t], dev)
+        for t in range(tiles)
+        for slot, dev in ((1, zr), (2, zl))
+    }
+    for c in q_out.values():
+        c.start()
+    q_fwd = {}
+    for n in range(2 * tiles):
+        t, h = n // 2, n % 2
+        slot, dev = (1, zr) if n < tiles else (2, zl)
+        q_fwd[(t, h)] = remote(qb.at[slot, t, h], qb.at[3, t, h], qf_send.at[t, h], qf_recv.at[t, h], dev)
+
     kvp[WINDOW : WINDOW + rows] = kvw[...]
     wq = pacc[:, 1280:1408] * row_scale
     for t in range(tiles):
         qwt[t] = wq[QT * t : QT * t + QT].T.astype(bf16).reshape(2, 64, QT)
-    q_fwd = [
-        remote(qb.at[1, 0], qb.at[3, 0], qf_send.at[0], qf_recv.at[0], zr),
-        remote(qb.at[2, 1], qb.at[3, 1], qf_send.at[1], qf_recv.at[1], zl),
-    ]
     k_fwd = [
         remote(kvb.at[1, pl.ds(0, half)], kvb.at[3, pl.ds(0, half)], kf_send.at[0], kf_recv.at[0], xr),
         remote(kvb.at[2, pl.ds(half, half)], kvb.at[3, pl.ds(half, half)], kf_send.at[1], kf_recv.at[1], xl),
@@ -281,72 +282,77 @@
         keys = [(2, 0), (2, 1), (1, 0), (3, 0), (1, 1), (3, 1), (0, 0)]
         return [piece(part, src, d, cc) for d, cc in keys]
 
-    S = ((s00, s01), (s10, s11))
-    X = ((x00, x01), (x10, x11))
-
-    def stage_a(k, q, t, slot):
+    S = ((s00, s01), (s10, s11), (s20, s21), (s30, s31))
+    X = ((x00, x01), (x10, x11), (x20, x21), (x30, x31))
+
+    def stage_a(k, q, t, slot, h):
         z64, z96 = jnp.zeros((64, QT), bf16), jnp.zeros((96, QT), bf16)
         keys = jnp.concatenate([kvb[k, 0:rows], rotx[k]], axis=1)
-        for h in range(2):
-            qq = qb[q, h, t]
-            if h == 0:
-                parts = [qq[0:64], z64, qq[64:96], z96]
-            else:
-                parts = [z64, qq[0:64], qq[64:96], z96]
-            s = jnp.dot(keys, jnp.concatenate(parts, axis=0), preferred_element_type=f32)
-            S[slot][h][...] = s
-            X[slot][h][...] = jnp.max(s.reshape(rows // 8, 8, QT), axis=0)
-
-    def stage_b(k, q, t, slot):
-        for h in range(2):
-            old = mref[q, t, h : h + 1]
-            new = jnp.maximum(old, jnp.max(X[slot][h][...], axis=0, keepdims=True))
-            alpha = jnp.exp2(old - new)
-            mref[q, t, h : h + 1] = new
-            total = None
-            for c in range(rows // 256):
-                p = jnp.exp2(S[slot][h][c * 256 : (c + 1) * 256] - new).astype(bf16)
-                base = rows + quarter + 256 * c + 64 * h
-                v = jnp.concatenate([kvb[k, base : base + 64], kvb[k, base + 128 : base + 192]], axis=1)
-                v = jnp.concatenate([v, jnp.ones((16, 256), bf16)], axis=0)
-                o = jnp.dot(v, p, preferred_element_type=f32)
-                total = o if total is None else total + o
-            lref[q, t, h : h + 1] = lref[q, t, h : h + 1] * alpha + total[64:65]
-            acc[q, t, 64 * h : 64 * h + 64] = acc[q, t, 64 * h : 64 * h + 64] * alpha + total[0:64]
+        qq = qb[q, t, h]
+        parts = [z64, z64, qq[64:96], z96]
+        parts[h] = qq[0:64]
+        s = jnp.dot(keys, jnp.concatenate(parts, axis=0), preferred_element_type=f32)
+        S[slot][h][...] = s
+        X[slot][h][...] = jnp.max(s.reshape(rows // 8, 8, QT), axis=0)
+
+    def stage_b(k, q, t, slot, h):
+        old = mref[q, t, h : h + 1]
+        new = jnp.maximum(old, jnp.max(X[slot][h][...], axis=0, keepdims=True))
+        alpha = jnp.exp2(old - new)
+        mref[q, t, h : h + 1] = new
+        total = None
+        for lo in range(0, rows, PV):
+            hi = min(rows, lo + PV)
+            p = jnp.exp2(S[slot][h][lo:hi] - new).astype(bf16)
+            base = rows + quarter + 64 * h
+            v = jnp.concatenate([kvb[k, base + c : base + c + 64] for c in range(lo, hi, 128)], axis=1)
+            v = jnp.concatenate([v, jnp.ones((16, hi - lo), bf16)], axis=0)
+            o = jnp.dot(v, p, preferred_element_type=f32)
+            total = o if total is None else total + o
+        lref[q, t, h : h + 1] = lref[q, t, h : h + 1] * alpha + total[64:65]
+        acc[q, t, 64 * h : 64 * h + 64] = acc[q, t, 64 * h : 64 * h + 64] * alpha + total[0:64]
 
     def pipeline(n, where, before=None, after=None):
-        def A(i, slot):
-            stage_a(*where(i), slot)
-
-        def B(i, slot):
-            stage_b(*where(i), slot)
-            if after is not None:
-                after(i)
-
-        A(0, 0)
-        loops = (n - 1) // 2
-
-        @pl.loop(0, loops)
-        def _(j):
-            i = 2 * j
-            if before is not None:
-                before(i + 1)
-            A(i + 1, 1)
-            B(i, 0)
-            if before is not None:
-                before(i + 2)
-            A(i + 2, 0)
-            B(i + 1, 1)
-
-        i = 2 * loops
-        if n % 2 == 0:
-            if before is not None:
-                before(i + 1)
-            A(i + 1, 1)
-            B(i, 0)
-            B(i + 1, 1)
-        else:
-            B(i, 0)
+        def step(first, second):
+            for i, _ in first:
+                if before is not None:
+                    before(i)
+            for d in range(2):
+                for h in range(2):
+                    if d < len(first):
+                        i, slot = first[d]
+                        stage_a(*where(i), slot, h)
+                    if d < len(second):
+                        i, slot = second[d]
+                        stage_b(*where(i), slot, h)
+            for i, _ in second:
+                if after is not None:
+                    after(i)
+
+        def body(i, at):
+            step(
+                [(i + 2, (at + 2) % 4), (i + 3, (at + 3) % 4)], [(i, at), (i + 1, at + 1)]
+            )
+
+        step([(0, 0), (1, 1)], [])
+        bodies = n // 2 - 1
+        loops = bodies // 2
+        if loops == 1:
+            body(0, 0)
+            body(2, 2)
+        elif loops:
+            @pl.loop(0, loops)
+            def _(j):
+                body(4 * j, 0)
+                body(4 * j + 2, 2)
+        if bodies % 2:
+            body(4 * loops, 0)
+        i = 2 * bodies
+        last = [(i, i % 4), (i + 1, (i + 1) % 4)]
+        if n % 2:
+            step([(i + 2, (i + 2) % 4)], last)
+            last = [(i + 2, (i + 2) % 4)]
+        step([], last)
 
     def window():
         for c in halo:
@@ -377,42 +383,46 @@
             osw[pl.ds(pl.multiple_of(t * QT, QT), QT), :] = S[0][0][0:128].T.astype(bf16)
 
     unpack(0)
-
-    @pl.loop(0, 3)
-    def _(q):
-        @pl.when(q == 1)
-        def _():
-            window()
-            for c in pieces(0, osw):
-                c.start()
-            orow[0, core, 0] = osw[pl.ds(pl.multiple_of(tp * mine, mine), mine), :]
-            for c, f in ((q_out[(0, 0)], q_fwd[0]), (q_out[(1, 1)], q_fwd[1])):
-                c.wait_recv()
-                f.start()
-            q_out[(0, 1)].wait_recv()
-
-        @pl.when(q == 2)
-        def _():
-            q_out[(1, 0)].wait_recv()
-            for c, f in ((k_out[(0, 0)], k_fwd[0]), (k_out[(1, 1)], k_fwd[1])):
-                c.wait_recv()
-                f.start()
-
-        pipeline(tiles, lambda i: (0, q, i))
+    pipeline(tiles, lambda i: (0, 0, i))
+    window()
+    for c in pieces(0, osw):
+        c.start()
+    orow[0, core, 0] = osw[pl.ds(pl.multiple_of(tp * mine, mine), mine), :]
+
+    def queries_arrive(i):
+        if i % 2 == 0:
+            t = i // 2
+            q_out[(1, t)].wait_recv()
+            q_out[(2, t)].wait_recv()
+            for h in range(2):
+                q_fwd[(t, h)].start()
+            if t == tiles - 1:
+                for c, f in ((k_out[(0, 0)], k_fwd[0]), (k_out[(1, 1)], k_fwd[1])):
+                    c.wait_recv()
+                    f.start()
+
+    pipeline(2 * tiles, lambda i: (0, 1 + i % 2, i // 2), queries_arrive)
 
     k_out[(0, 1)].wait_recv()
     k_out[(1, 0)].wait_recv()
     unpack(1)
     unpack(2)
-    for c in q_fwd:
+    for c in q_fwd.values():
         c.wait_recv()
+    wts.arrive(1, 0)
+    wts.arrive(2, 1)
 
     def arrive(i):
-        @pl.when(i == 3 * tiles)
+        @pl.when(i == 5 * tiles)
         def _():
             for c in k_fwd:
                 c.wait_recv()
             unpack(3)
+
+        @pl.when(i == 6 * tiles)
+        def _():
+            wts.arrive(1, 1)
+            wts.arrive(2, 0)
 
     def finish(q, t):
         for h in range(2):
@@ -428,35 +438,35 @@
             remote(ssend.at[q, t], sbuf.at[slot, t], s_send.at[q, t], s_recv.at[slot, t], dev),
         )
 
-    pipeline(4 * tiles, lambda i: (i // tiles, 3, i % tiles), arrive)
-    for t in range(tiles):
-        finish(3, t)
-    for t in range(tiles):
-        for c in back(3, t):
-            c.start()
-    wts.arrive(1, 0)
-    wts.arrive(2, 1)
-
-    @pl.loop(0, 3)
-    def _(r):
-        q = 2 - r
-
-        def done(i):
-            @pl.when(i % 3 == 2)
+    def mixed_order(i):
+        p = i // tiles
+        return p - 2 * (p // 3) + p // 6, 3 - p // 3 + p // 5, i % tiles
+
+    def give_back(i):
+        for q in (3, 2):
+            @pl.when(i // tiles == 8 - q)
             def _():
-                finish(q, i // 3)
-                for n in (0, 1):
-                    @pl.when(r == n)
-                    def _():
-                        for c in back(2 - n, i // 3):
-                            c.start()
-
-        pipeline(3 * tiles, lambda i: (1 + i % 3, q, i // 3), after=done)
-
-        @pl.when(r == 1)
+                finish(q, i % tiles)
+                for c in back(q, i % tiles):
+                    c.start()
+
+    pipeline(7 * tiles, mixed_order, arrive, give_back)
+
+    def by_tile(i):
+        return 1 + i % 3, 1 - i // (3 * tiles), (i % (3 * tiles)) // 3
+
+    def give_back_last(i):
+        @pl.when(i % 3 == 2)
         def _():
-            wts.arrive(1, 1)
-            wts.arrive(2, 0)
+            _, q, t = by_tile(i)
+            finish(q, t)
+
+            @pl.when(i < 3 * tiles)
+            def _():
+                for c in back(1, t):
+                    c.start()
+
+    pipeline(6 * tiles, by_tile, None, give_back_last)
 
     for q in (3, 2, 1):
         for t in range(tiles):
@@ -483,26 +493,34 @@
     orow[0, core, 1] = osl[pl.ds(pl.multiple_of(tp * mine, mine), mine), :]
     wts.arrive(3, 0)
     wts.arrive(3, 1)
-    for s in range(4):
-        for p in (0, 1):
-            wts.partner(s, p)
-            for cc in (0, 1) if s else (1 - core,):
-                there = orow.at[s, cc, p]
-                remote(there, there, a_send.at[p, 0], a_recv.at[p, s, cc], partner).wait_recv()
-
-    @pl.loop(0, D // 512)
-    def _(b):
-        cols = pl.ds(pl.multiple_of(b * 512, 512), 512)
-        total = None
-        for s in range(4):
-            for cc in (0, 1):
-                o = jnp.concatenate([orow[s, cc, 0], orow[s, cc, 1]], axis=1)
-                w = jnp.concatenate([wb[s, cc, 0, :, cols], wb[s, cc, 1, :, cols]], axis=0)
-                g = jnp.dot(o, w, preferred_element_type=f32).astype(bf16).astype(f32)
-                total = g if total is None else total + g
-        result[:, cols] = total.astype(bf16)
-
-    for c in halo + list(q_out.values()) + list(k_out.values()) + q_fwd + k_fwd:
+
+    def output(slots, last):
+        for s in slots:
+            for p in (0, 1):
+                wts.partner(s, p)
+                for cc in (0, 1) if s else (1 - core,):
+                    there = orow.at[s, cc, p]
+                    remote(there, there, a_send.at[p, 0], a_recv.at[p, s, cc], partner).wait_recv()
+
+        @pl.loop(0, D // 512)
+        def _(b):
+            cols = pl.ds(pl.multiple_of(b * 512, 512), 512)
+            total = facc[:, cols] if last else None
+            for s in slots:
+                for cc in (0, 1):
+                    o = jnp.concatenate([orow[s, cc, 0], orow[s, cc, 1]], axis=1)
+                    w = jnp.concatenate([wb[s, cc, 0, :, cols], wb[s, cc, 1, :, cols]], axis=0)
+                    g = jnp.dot(o, w, preferred_element_type=f32).astype(bf16).astype(f32)
+                    total = g if total is None else total + g
+            if last:
+                result[:, cols] = total.astype(bf16)
+            else:
+                facc[:, cols] = total
+
+    output((0, 1, 2), False)
+    output((3,), True)
+
+    for c in halo + list(q_out.values()) + list(k_out.values()) + list(q_fwd.values()) + k_fwd:
         c.wait_send()
     for q in (3, 2, 1):
         for t in range(tiles):
@@ -550,11 +568,11 @@
             V((32, 128), f32), V((32, rows), f32), V((rows, 1664), f32), V((rows, 128), f32),
             V((message, 128), bf16), V((tiles, 2, 64, QT), bf16), V((rows, 128), bf16),
             V((rows, 128), bf16), V((rows, 128), bf16), V((4, 2, 2, mine, 128), bf16),
-            V((4, message, 128), bf16), V((4, rows, 128), bf16), V((4, 2, tiles, 96, QT), bf16),
+            V((4, message, 128), bf16), V((4, rows, 128), bf16), V((4, tiles, 2, 96, QT), bf16),
             V((rows + 2 * WINDOW, 128), bf16),
             V((4, tiles, 8, QT), f32), V((4, tiles, 8, QT), f32), V((4, tiles, 128, QT), f32),
         ]
-        + [V((rows, QT), f32)] * 4 + [V((8, QT), f32)] * 4
+        + [V((rows, QT), f32)] * 8 + [V((8, QT), f32)] * 8 + [V((mine, D), f32)]
         + [
             V((4, tiles, 128, QT), bf16), V((4, tiles, 8, QT), f32),
             V((4, tiles, 128, QT), bf16), V((4, tiles, 8, QT), f32),
@@ -563,7 +581,7 @@
         + gather_sems + gather_sems
         + [
             dma((2, 8)), dma((2, 4, 2)),
-            dma((2,)), dma((2,)), dma((2, 2)), dma((2, 2)), dma((2,)), dma((2,)),
+            dma((2,)), dma((2,)), dma((3, tiles)), dma((3, tiles)), dma((tiles, 2)), dma((tiles, 2)),
             dma((2, 2)), dma((2, 2)), dma((2,)), dma((2,)),
             dma((4, tiles)), dma((4, tiles)), dma((4, tiles)), dma((4, tiles)),
         ],

time: 77.4 us -> 73.5 us (0.950)
  Pallas kernels: 75.5 us -> 71.5 us
    pallas_call x1, Pallas kernels: 75.5 us -> 71.5 us  [per_device(): pl.pallas_call(functools.partial(layer_kernel, rows, nsp // NX, NX, ntp /...]
where the time goes in v4:
time: 73.5 us; the launch traced here: 73.3 us
  Pallas kernels  71.5 us (97%)
  local copies, waits for them, and re-layouts  1.77 us (2%)
    pallas_call x1, Pallas kernels, per_device(): pl.pallas_call(functools.partial(layer_kernel, rows, nsp // NX, NX, ntp /...  71.5 us
    unnamed x1, local copies, waits for them, and re-layouts  1.77 us

profile of v4, /device:TPU:1, one launch (start us, length us, event | category | flops | bytes accessed | tf_op | source)
XLA Modules:
  0.0 73.3 jit_solution(2837842958778088685)
XLA Ops:
  0.0 71.5 %layer.1 = bf16[96,2048]{1,0:T(8,128)(2,1)} custom-call(bf16[768,256]{1,0:T(8,128)(2,1)} %tokens.1, f32[1,2048]{1,0:T(1,128)} %bitcast.11, f32[6,128]{1,0:T(8,128)} %bitcast.12, f32[1,512]{1,0:T(1,128)} %bitcast.13, f32[2]{0:T(128)} %sinks.1, f32[16]{0:T(128)} %constant.6.clone.slopes, bf16[2048,128]{1,0:T(8,128)(2,1)} %w_query.1, bf16[64,2048]{1,0:T(8,128)(2,1)} %bitcast.8, ...), custom_call_target="tpu_custom_call" | custom-call | tf_op jit(solution)/shard_map/layer/pallas_call | solution.py:558
  71.6 1.8 %copy.21 = bf16[96,2048]{1,0:T(8,128)(2,1)} copy(bf16[96,2048]{1,0:T(8,128)(2,1)} %layer.1) | data formatting | bytes 786432

commit v5 on v4

--- a/solution.py
+++ b/solution.py
@@ -19,6 +19,7 @@
 NEG = -1e30
 NX = 4
 PV = 768
+CB = 512
 
 
 def remote(src, dst, ss, rs, dev):
@@ -28,18 +29,27 @@
 
 
 class ChipGather:
-    def __init__(self, own, buf, core, right, left, partner, sems):
+    def __init__(self, own, buf, core, right, left, partner, sems, keep):
         ysend, yrecv, fsend, psend, precv = sems
         self.own, self.buf, self.core = own, buf, core
+        size = buf.shape[3]
+        head, rest = pl.ds(0, keep), pl.ds(keep, size - keep)
         self.out = {
             (s, p): remote(own[p], buf.at[s, core, p], ysend.at[s, p], yrecv.at[s, p], dev)
             for s, dev in ((1, right), (2, left))
             for p in (0, 1)
         }
         self.fwd = {
-            (3, 0): remote(buf.at[1, core, 0], buf.at[3, core, 0], fsend.at[0], yrecv.at[3, 0], right),
+            (3, 0): remote(
+                buf.at[1, core, 0, head], buf.at[3, core, 0, head], fsend.at[0], yrecv.at[3, 0], right
+            ),
             (3, 1): remote(buf.at[2, core, 1], buf.at[3, core, 1], fsend.at[1], yrecv.at[3, 1], left),
         }
+        self.more = []
+        if keep < size:
+            self.more = [
+                remote(buf.at[2, core, 0, rest], buf.at[3, core, 0, rest], fsend.at[2], yrecv.at[0, 0], left)
+            ]
         self.relay = {
             (s, p): remote(
                 own[p] if s == 0 else buf.at[s, core, p], buf.at[s, core, p],
@@ -61,6 +71,12 @@
             self.fwd[(3, 0)].start()
         if (slot, part) == (2, 1):
             self.fwd[(3, 1)].start()
+        if (slot, part) == (2, 0):
+            for c in self.more:
+                c.start()
+        if (slot, part) == (3, 0):
+            for c in self.more:
+                c.wait_recv()
         if relay:
             self.relay[(slot, part)].start()
 
@@ -68,7 +84,71 @@
         self.relay[(slot, part)].wait_recv()
 
     def drain(self):
-        for c in list(self.out.values()) + list(self.fwd.values()) + list(self.relay.values()):
+        for c in list(self.out.values()) + list(self.fwd.values()) + self.more + list(self.relay.values()):
+            c.wait_send()
+
+
+class WeightGather:
+    def __init__(self, buf, core, a, right, left, partner, across, sems):
+        osend, orecv, fsend, frecv, xsend, xrecv, psend, precv = sems
+        rows = buf.shape[3]
+        b, cut, mid = 1 - a, rows // 4, rows // 2
+        chunks = ((a, pl.ds(0, rows)), (b, pl.ds(0, cut)), (b, pl.ds(cut, rows - cut)))
+        self.out = {
+            (s, i): remote(
+                buf.at[0, core, p, r], buf.at[s, core, p, r], osend.at[s, i], orecv.at[s, i], dev
+            )
+            for s, dev in ((1, right), (2, left))
+            for i, (p, r) in enumerate(chunks)
+        }
+        self.fwd = [
+            remote(buf.at[s, core, a, r], buf.at[3, core, a, r], fsend.at[i], frecv.at[i], dev)
+            for i, (s, dev, r) in enumerate(((1, right, pl.ds(0, mid)), (2, left, pl.ds(mid, rows - mid))))
+        ]
+        self.swap = remote(buf.at[3, core, a], buf.at[3, core, a], xsend.at[0], xrecv.at[0], across)
+        self.relay = {
+            (s, i): remote(
+                buf.at[s, core, p], buf.at[s, core, p], psend.at[s, i], precv.at[s, i], partner
+            )
+            for s in range(4)
+            for i, p in enumerate((a, b))
+        }
+
+    def start(self):
+        for key in ((1, 0), (2, 0), (1, 1), (2, 1)):
+            self.out[key].start()
+        for i in (0, 1):
+            self.relay[(0, i)].start()
+
+    def first(self):
+        for s in (1, 2):
+            self.out[(s, 0)].wait_recv()
+            self.fwd[s - 1].start()
+        for s in (1, 2):
+            self.out[(s, 2)].start()
+            self.relay[(s, 0)].start()
+
+    def second(self):
+        for c in self.fwd:
+            c.wait_recv()
+        self.swap.start()
+        self.relay[(3, 0)].start()
+
+    def third(self):
+        for s in (1, 2):
+            self.out[(s, 1)].wait_recv()
+            self.out[(s, 2)].wait_recv()
+            self.relay[(s, 1)].start()
+
+    def fourth(self):
+        self.swap.wait_recv()
+        self.relay[(3, 1)].start()
+
+    def partner(self, slot, part):
+        self.relay[(slot, part)].wait_recv()
+
+    def drain(self):
+        for c in list(self.out.values()) + self.fwd + [self.swap] + list(self.relay.values()):
             c.wait_send()
 
 
@@ -76,15 +156,15 @@
     rows, nz, nx, ny,
     tokens, norm_gain, query_gain, latent_gain, sinks, slopes,
     w_query, w_key, w_value, d_query, d_latent, w_rot, u_query, u_key, u_value, o_window, o_latent,
-    tab_far, tab_near,
+    tab_far, tab_near, tab_near_q,
     result,
-    tb, wb, wdq, wdl, wcat, wnarrow, uq, uk, uv, far, near, pacc, sq,
+    tb, wb, wdq, wdl, wcat, wnarrow, uq, uk, uv, far, near, near_q, pacc, sq,
     kvm, qwt, kvw, osw, osl, orow,
     kvb, rotx, qb, kvp, mref, lref, acc,
-    s00, s01, s10, s11, s20, s21, s30, s31, x00, x01, x10, x11, x20, x21, x30, x31, facc,
+    s00, s01, s10, s11, s20, s21, s30, s31, x00, x01, x10, x11, x20, x21, x30, x31, facc, total_out,
     osend, ssend, obuf, sbuf,
-    l_sem, t_ysend, t_yrecv, t_fsend, t_psend, t_precv, w_ysend, w_yrecv, w_fsend, w_psend, w_precv,
-    a_send, a_recv,
+    l_sem, t_ysend, t_yrecv, t_fsend, t_psend, t_precv, w_osend, w_orecv, w_fsend, w_frecv, w_xsend, w_xrecv, w_psend, w_precv,
+    a_send, a_recv, r_sem,
     h_send, h_recv, q_send, q_recv, qf_send, qf_recv, k_send, k_recv, kf_send, kf_recv,
     o_send, o_recv, s_send, s_recv,
 ):
@@ -103,7 +183,7 @@
             (d_query, wdq), (d_latent, wdl), (w_query, wcat.at[:, pl.ds(0, 128)]),
             (w_key, wnarrow.at[pl.ds(0, 64)]), (w_value, wnarrow.at[pl.ds(64, 64)]),
             (w_rot, wnarrow.at[pl.ds(128, 32)]), (u_query, uq), (u_key, uk), (u_value, uv),
-            (tab_far.at[sp], far), (tab_near, near),
+            (tab_far.at[sp], far), (tab_near, near), (tab_near_q, near_q),
             (o_window, wb.at[0, core, 0]), (o_latent, wb.at[0, core, 1]),
         ))
     ]
@@ -130,11 +210,11 @@
 
     tok = ChipGather(
         [tokens.at[pl.ds(p * half_rows, half_rows)] for p in (0, 1)], tb, core,
-        chip(1, core), chip(ny - 1, core), partner, (t_ysend, t_yrecv, t_fsend, t_psend, t_precv),
+        chip(1, core), chip(ny - 1, core), partner, (t_ysend, t_yrecv, t_fsend, t_psend, t_precv), half_rows,
     )
-    wts = ChipGather(
-        [o_window, o_latent], wb, core,
-        chip(1, core), chip(ny - 1, core), partner, (w_ysend, w_yrecv, w_fsend, w_psend, w_precv),
+    wts = WeightGather(
+        wb, core, x % 2, chip(1, core), chip(ny - 1, core), partner, at(z, x + 1 - 2 * (x % 2)),
+        (w_osend, w_orecv, w_fsend, w_frecv, w_xsend, w_xrecv, w_psend, w_precv),
     )
     tok.start()
     for p in (0, 1):
@@ -155,16 +235,29 @@
         at_b = pl.ds(pl.multiple_of(b * 128, 128), 128)
         wcat[at_b, 128:384] = wnarrow[:, at_b].astype(f32).T.astype(bf16)
 
-    arrivals = {(1, 0): ((1, 0), (2, 1)), (1, 1): ((1, 1), (2, 0)), (3, 0): ((3, 0), (3, 1))}
-
-    @pl.loop(0, 4)
+    arrivals = {(1, 0): ((1, 0), (2, 1)), (1, 1): ((1, 1), (2, 0))}
+
+    all_parts = ((wdl, 768, 1280), (wcat, 1280, 1664), (wdq, 0, 768))
+
+    def unit(t32, w_rows, out_rows, parts=all_parts, count=True):
+        if count:
+            squares = t32 * t32
+            part_sq = squares[:, 0:128]
+            for lo in range(128, t32.shape[1], 128):
+                part_sq = part_sq + squares[:, lo : lo + 128]
+            sq[out_rows] += part_sq
+        scaled = (t32 * norm_gain[:, w_rows]).astype(bf16)
+        for w, lo, hi in parts:
+            pacc[out_rows, lo:hi] += jnp.dot(scaled, w[w_rows, :], preferred_element_type=f32)
+
+    @pl.loop(0, 3)
     def _(slot):
-        chip_at = (y + ny - (slot + slot // 2 - 2 * (slot // 3))) % ny
+        chip_at = (y + ny - (slot + slot // 2)) % ny
         w_rows = pl.ds(pl.multiple_of(chip_at * 512, 512), 512)
 
         @pl.loop(0, 2)
         def _(part):
-            for s in range(4):
+            for s in range(3):
                 for p in (0, 1):
                     @pl.when((slot == s) & (part == p))
                     def _():
@@ -173,22 +266,34 @@
                         if (s, p) == (1, 1):
                             wts.start()
                         tok.partner(s, p)
+            out_rows = pl.ds(pl.multiple_of(part * half_rows, half_rows), half_rows)
             t32 = jnp.concatenate([tb[slot, 0, part], tb[slot, 1, part]], axis=1).astype(f32)
+            unit(t32, w_rows, out_rows)
+
+    tok.arrive(3, 0)
+    tok.arrive(3, 1)
+
+    @pl.loop(0, 2)
+    def _(turn):
+        from_core = core + turn - 2 * core * turn
+
+        @pl.when(turn == 1)
+        def _():
+            tok.partner(3, 0)
+            tok.partner(3, 1)
+
+        @pl.loop(0, 2)
+        def _(part):
+            w_rows = pl.ds(pl.multiple_of(((y + 2) % ny) * 512 + from_core * 256, 256), 256)
             out_rows = pl.ds(pl.multiple_of(part * half_rows, half_rows), half_rows)
-            squares = t32 * t32
-            sq[out_rows] += (
-                squares[:, 0:128] + squares[:, 128:256] + squares[:, 256:384] + squares[:, 384:512]
-            )
-            scaled = (t32 * norm_gain[:, w_rows]).astype(bf16)
-            for w, lo, hi in ((wdl, 768, 1280), (wcat, 1280, 1664), (wdq, 0, 768)):
-                pacc[out_rows, lo:hi] += jnp.dot(scaled, w[w_rows, :], preferred_element_type=f32)
+            unit(tb[3, from_core, part].astype(f32), w_rows, out_rows, all_parts[:2])
 
     cos_f, sin_f = far[0:16, 0:1], far[16:32, 0:1]
-    cos_n, sin_n = near[0:16, :], near[16:32, :]
-    cos = cos_f * cos_n - sin_f * sin_n
-    sin = sin_f * cos_n + cos_f * sin_n
-    near[0:16, :] = cos
-    near[16:32, :] = sin
+    for table in (near, near_q):
+        cos_n, sin_n = table[0:16, :], table[16:32, :]
+        cos, sin = cos_f * cos_n - sin_f * sin_n, sin_f * cos_n + cos_f * sin_n
+        table[0:16, :] = cos
+        table[16:32, :] = sin
     row_scale = lax.rsqrt(jnp.sum(sq[...], axis=1, keepdims=True) * (1.0 / D) + EPS)
 
     def normed(lo, hi, gain):
@@ -203,26 +308,34 @@
     ]
     for c in halo:
         c.start()
-    quarter = rows // 4
+    quarter, eighth = rows // 4, rows // 8
+    half = kvm.shape[0] // 2
+    v_at = half_rows + eighth
+
+    def value_row(c):
+        return (c // half_rows) * half + v_at + c % half_rows
+
     up_kv = jnp.concatenate([uk[...], uv[...]], axis=1)
     kv = jnp.dot(normed(768, 1280, latent_gain[...]), up_kv, preferred_element_type=f32)
-    kvm[0:rows] = kv[:, 0:128].astype(bf16)
+    for e in (0, 1):
+        kvm[e * half : e * half + half_rows] = kv[e * half_rows : (e + 1) * half_rows, 0:128].astype(bf16)
     for b in range(rows // 128):
         block = kv[128 * b : 128 * b + 128, 128:256].T
-        kvm[rows + quarter + 128 * b : rows + quarter + 128 * b + 128] = block.astype(bf16)
+        kvm[value_row(128 * b) : value_row(128 * b) + 128] = block.astype(bf16)
     rr = (pacc[:, 1536:1664] * row_scale).astype(bf16).astype(f32).T
     ra, rb = rr[0:16], rr[16:32]
     cos, sin = near[0:16, :], near[16:32, :]
     turned = jnp.concatenate([ra * cos - rb * sin, rb * cos + ra * sin, jnp.zeros((96, rows), f32)], axis=0).T
-    packed = turned[0:quarter]
-    for g in range(1, 4):
-        packed = packed + pltpu.roll(turned[g * quarter : (g + 1) * quarter], 32 * g, 1)
-    kvm[rows : rows + quarter] = packed.astype(bf16)
-    half = kvm.shape[0] // 2
+    for e in (0, 1):
+        packed = turned[e * half_rows : e * half_rows + eighth]
+        for g in range(1, 4):
+            lo = e * half_rows + g * eighth
+            packed = packed + pltpu.roll(turned[lo : lo + eighth], 32 * g, 1)
+        kvm[e * half + half_rows : e * half + v_at] = packed.astype(bf16)
     k_out = {}
     for order in ((0, 1), (1, 0)):
         for which, h in ((0, order[0]), (1, order[1])):
-            slot, dev = ((1, xr), (2, xl))[which]
+            slot, dev = 1 if which == h else 2, (xr, xl)[which]
             k_out[(which, h)] = remote(
                 kvm.at[pl.ds(h * half, half)], kvb.at[slot, pl.ds(h * half, half)],
                 k_send.at[which, h], k_recv.at[which, h], dev,
@@ -231,9 +344,20 @@
         k_out[key].start()
     kvb[0] = kvm[...]
 
-    qf = lax.dot_general(
-        uq[...], normed(0, 768, jnp.concatenate([query_gain[i : i + 1] for i in range(6)], axis=1)), (((1,), (1,)), ((), ())), preferred_element_type=f32
-    ) * (LOG2E * 96 ** (-0.5))
+    @pl.loop(0, 2)
+    def _(part):
+        w_rows = pl.ds(pl.multiple_of(((y + 2) % ny) * 512, 512), 512)
+        out_rows = pl.ds(pl.multiple_of(part * half_rows, half_rows), half_rows)
+        t32 = jnp.concatenate([tb[3, 0, part], tb[3, 1, part]], axis=1).astype(f32)
+        unit(t32, w_rows, out_rows, all_parts[2:], False)
+
+    sub = mine // tiles
+    nq = normed(0, 768, jnp.concatenate([query_gain[i : i + 1] for i in range(6)], axis=1))
+    nq = jnp.concatenate(
+        [nq[mine * j + sub * t : mine * j + sub * t + sub] for t in range(tiles) for j in range(ntp)], axis=0
+    )
+    qf = lax.dot_general(uq[...], nq, (((1,), (1,)), ((), ())), preferred_element_type=f32) * (LOG2E * 96 ** (-0.5))
+    cos, sin = near_q[0:16, :], near_q[16:32, :]
     for h in range(2):
         a, b = qf[96 * h + 64 : 96 * h + 80], qf[96 * h + 80 : 96 * h + 96]
         whole = jnp.concatenate(
@@ -260,34 +384,45 @@
         qwt[t] = wq[QT * t : QT * t + QT].T.astype(bf16).reshape(2, 64, QT)
     k_fwd = [
         remote(kvb.at[1, pl.ds(0, half)], kvb.at[3, pl.ds(0, half)], kf_send.at[0], kf_recv.at[0], xr),
-        remote(kvb.at[2, pl.ds(half, half)], kvb.at[3, pl.ds(half, half)], kf_send.at[1], kf_recv.at[1], xl),
+        remote(kvb.at[1, pl.ds(half, half)], kvb.at[3, pl.ds(half, half)], kf_send.at[1], kf_recv.at[1], xl),
     ]
 
     def unpack(i):
-        packed = kvb[i, rows : rows + quarter].astype(f32)
-        for g in range(4):
-            moved = packed if g == 0 else pltpu.roll(packed, 128 - 32 * g, 1)
-            rotx[i, g * quarter : (g + 1) * quarter] = moved.astype(bf16)
-
-    def piece(part, src, d, cc):
-        dev = chip(d, cc) if d else partner
-        slot = (0, 1, 3, 2)[d]
-        row_at = pl.ds(pl.multiple_of(dev[1] * mine, mine), mine)
-        i = 2 * d + (cc if d else 0)
-        return remote(
-            src.at[row_at], orow.at[slot, core, part], a_send.at[part, i], a_recv.at[part, slot, core], dev
-        )
-
-    def pieces(part, src):
-        keys = [(2, 0), (2, 1), (1, 0), (3, 0), (1, 1), (3, 1), (0, 0)]
-        return [piece(part, src, d, cc) for d, cc in keys]
+        for e in (0, 1):
+            packed = kvb[i, e * half + half_rows : e * half + v_at].astype(f32)
+            for g in range(4):
+                moved = packed if g == 0 else pltpu.roll(packed, 128 - 32 * g, 1)
+                lo = e * half_rows + g * eighth
+                rotx[i, lo : lo + eighth] = moved.astype(bf16)
+
+    def pieces(part, t=0):
+        found = []
+        for d, cc in ((2, 0), (2, 1), (1, 0), (3, 0), (1, 1), (3, 1), (0, 0)):
+            dev = chip(d, cc) if d else partner
+            slot = (0, 1, 3, 2)[d]
+            src, dst = piece_refs(part, t, dev[1], slot)
+            found.append(remote(src, dst, a_send.at[part + t, 2 * d + cc], a_recv.at[part + t, slot, core], dev))
+        return found
+
+    def piece_refs(part, t, owner, slot):
+        if part == 0:
+            return osw.at[pl.ds(pl.multiple_of(owner * mine, mine), mine)], orow.at[slot, core, 0]
+        row_at = pl.multiple_of(t * QT + owner * sub, sub)
+        there = pl.ds(pl.multiple_of(t * sub, sub), sub)
+        return osl.at[pl.ds(row_at, sub)], orow.at[slot, core, 1, there]
+
+    def piece_there(part, t, slot, cc):
+        if part == 0:
+            return orow.at[slot, cc, 0]
+        return orow.at[slot, cc, 1, pl.ds(t * sub, sub)]
 
     S = ((s00, s01), (s10, s11), (s20, s21), (s30, s31))
     X = ((x00, x01), (x10, x11), (x20, x21), (x30, x31))
 
     def stage_a(k, q, t, slot, h):
         z64, z96 = jnp.zeros((64, QT), bf16), jnp.zeros((96, QT), bf16)
-        keys = jnp.concatenate([kvb[k, 0:rows], rotx[k]], axis=1)
+        keys = jnp.concatenate([kvb[k, 0:half_rows], kvb[k, half : half + half_rows]], axis=0)
+        keys = jnp.concatenate([keys, rotx[k]], axis=1)
         qq = qb[q, t, h]
         parts = [z64, z64, qq[64:96], z96]
         parts[h] = qq[0:64]
@@ -304,8 +439,8 @@
         for lo in range(0, rows, PV):
             hi = min(rows, lo + PV)
             p = jnp.exp2(S[slot][h][lo:hi] - new).astype(bf16)
-            base = rows + quarter + 64 * h
-            v = jnp.concatenate([kvb[k, base + c : base + c + 64] for c in range(lo, hi, 128)], axis=1)
+            v_rows = [value_row(c) + 64 * h for c in range(lo, hi, 128)]
+            v = jnp.concatenate([kvb[k, r : r + 64] for r in v_rows], axis=1)
             v = jnp.concatenate([v, jnp.ones((16, hi - lo), bf16)], axis=0)
             o = jnp.dot(v, p, preferred_element_type=f32)
             total = o if total is None else total + o
@@ -385,9 +520,10 @@
     unpack(0)
     pipeline(tiles, lambda i: (0, 0, i))
     window()
-    for c in pieces(0, osw):
+    for c in pieces(0):
         c.start()
     orow[0, core, 0] = osw[pl.ds(pl.multiple_of(tp * mine, mine), mine), :]
+    wts.first()
 
     def queries_arrive(i):
         if i % 2 == 0:
@@ -403,26 +539,23 @@
 
     pipeline(2 * tiles, lambda i: (0, 1 + i % 2, i // 2), queries_arrive)
 
+    unpack(1)
+    pipeline(3 * tiles, lambda i: (1, i // tiles, i % tiles))
     k_out[(0, 1)].wait_recv()
     k_out[(1, 0)].wait_recv()
-    unpack(1)
     unpack(2)
     for c in q_fwd.values():
         c.wait_recv()
-    wts.arrive(1, 0)
-    wts.arrive(2, 1)
-
     def arrive(i):
-        @pl.when(i == 5 * tiles)
+        @pl.when(i == 4 * tiles)
         def _():
             for c in k_fwd:
                 c.wait_recv()
             unpack(3)
 
-        @pl.when(i == 6 * tiles)
+        @pl.when(i == 3 * tiles)
         def _():
-            wts.arrive(1, 1)
-            wts.arrive(2, 0)
+            wts.second()
 
     def finish(q, t):
         for h in range(2):
@@ -440,41 +573,22 @@
 
     def mixed_order(i):
         p = i // tiles
-        return p - 2 * (p // 3) + p // 6, 3 - p // 3 + p // 5, i % tiles
+        return p - p // 3 - p // 5, 3 - p // 3 + p // 4 - p // 5, i % tiles
 
     def give_back(i):
         for q in (3, 2):
-            @pl.when(i // tiles == 8 - q)
+            @pl.when(i // tiles == 7 - q)
             def _():
                 finish(q, i % tiles)
                 for c in back(q, i % tiles):
                     c.start()
 
-    pipeline(7 * tiles, mixed_order, arrive, give_back)
-
-    def by_tile(i):
-        return 1 + i % 3, 1 - i // (3 * tiles), (i % (3 * tiles)) // 3
-
-    def give_back_last(i):
-        @pl.when(i % 3 == 2)
-        def _():
-            _, q, t = by_tile(i)
-            finish(q, t)
-
-            @pl.when(i < 3 * tiles)
-            def _():
-                for c in back(1, t):
-                    c.start()
-
-    pipeline(6 * tiles, by_tile, None, give_back_last)
-
-    for q in (3, 2, 1):
-        for t in range(tiles):
+    pipeline(6 * tiles, mixed_order, arrive, give_back)
+
+    def combine(t):
+        for q in (3, 2, 1):
             for c in back(q, t):
                 c.wait_recv()
-
-    @pl.loop(0, tiles)
-    def _(t):
         ms = [ssend[0, t, 0:2]] + [sbuf[j, t, 0:2] for j in (1, 2, 3)]
         ls = [ssend[0, t, 2:4]] + [sbuf[j, t, 2:4] for j in (1, 2, 3)]
         top = jnp.maximum(jnp.maximum(ms[0], ms[1]), jnp.maximum(ms[2], ms[3]))
@@ -485,40 +599,70 @@
             total = osend[0, t, rows_h].astype(f32) * (ws[0] * inv)[h : h + 1]
             for j in (1, 2, 3):
                 total = total + obuf[j, t, rows_h].astype(f32) * (ws[j] * inv)[h : h + 1]
-            S[0][0][rows_h] = total
-        osl[pl.ds(pl.multiple_of(t * QT, QT), QT), :] = S[0][0][0:128].T.astype(bf16)
-
-    for c in pieces(1, osl):
-        c.start()
-    orow[0, core, 1] = osl[pl.ds(pl.multiple_of(tp * mine, mine), mine), :]
-    wts.arrive(3, 0)
-    wts.arrive(3, 1)
-
-    def output(slots, last):
+            facc[rows_h] = total
+        osl[pl.ds(pl.multiple_of(t * QT, QT), QT), :] = facc[...].T.astype(bf16)
+        for c in pieces(1, t):
+            c.start()
+        src, dst = piece_refs(1, t, tp, 0)
+        dst[...] = src[...]
+
+    def by_tile(i):
+        return 2 + i % 2, 1 - i // (2 * tiles), (i % (2 * tiles)) // 2
+
+    def give_back_last(i):
+        @pl.when(i % 2 == 1)
+        def _():
+            _, q, t = by_tile(i)
+            finish(q, t)
+
+            @pl.when(i < 2 * tiles)
+            def _():
+                for c in back(1, t):
+                    c.start()
+
+            @pl.when(i >= 2 * tiles)
+            def _():
+                combine(t)
+
+    def late(i):
+        @pl.when(i == 2 * tiles)
+        def _():
+            wts.third()
+
+    pipeline(4 * tiles, by_tile, late, give_back_last)
+
+    wts.fourth()
+    def weights_there(slots):
         for s in slots:
             for p in (0, 1):
                 wts.partner(s, p)
+
+    def heads_there(parts):
+        for part in parts:
+            for s in range(4):
                 for cc in (0, 1) if s else (1 - core,):
-                    there = orow.at[s, cc, p]
-                    remote(there, there, a_send.at[p, 0], a_recv.at[p, s, cc], partner).wait_recv()
-
-        @pl.loop(0, D // 512)
-        def _(b):
-            cols = pl.ds(pl.multiple_of(b * 512, 512), 512)
-            total = facc[:, cols] if last else None
-            for s in slots:
-                for cc in (0, 1):
-                    o = jnp.concatenate([orow[s, cc, 0], orow[s, cc, 1]], axis=1)
-                    w = jnp.concatenate([wb[s, cc, 0, :, cols], wb[s, cc, 1, :, cols]], axis=0)
-                    g = jnp.dot(o, w, preferred_element_type=f32).astype(bf16).astype(f32)
-                    total = g if total is None else total + g
-            if last:
-                result[:, cols] = total.astype(bf16)
-            else:
-                facc[:, cols] = total
-
-    output((0, 1, 2), False)
-    output((3,), True)
+                    there = piece_there(min(part, 1), part - 1, s, cc)
+                    remote(there, there, a_send.at[part, 0], a_recv.at[part, s, cc], partner).wait_recv()
+
+    weights_there(range(4))
+    heads_there(range(1 + tiles))
+    stores = [
+        pltpu.make_async_copy(
+            total_out.at[:, pl.ds(b * CB, CB)], result.at[:, pl.ds(b * CB, CB)], r_sem.at[b]
+        )
+        for b in range(D // CB)
+    ]
+    for b, store in enumerate(stores):
+        cols = pl.ds(b * CB, CB)
+        total = None
+        for s in range(4):
+            for cc in (0, 1):
+                o = jnp.concatenate([orow[s, cc, 0], orow[s, cc, 1]], axis=1)
+                w = jnp.concatenate([wb[s, cc, 0, :, cols], wb[s, cc, 1, :, cols]], axis=0)
+                g = jnp.dot(o, w, preferred_element_type=f32).astype(bf16).astype(f32)
+                total = g if total is None else total + g
+        total_out[:, cols] = total.astype(bf16)
+        store.start()
 
     for c in halo + list(q_out.values()) + list(k_out.values()) + list(q_fwd.values()) + k_fwd:
         c.wait_send()
@@ -526,11 +670,15 @@
         for t in range(tiles):
             for c in back(q, t):
                 c.wait_send()
-    for part, src in ((0, osw), (1, osl)):
-        for c in pieces(part, src):
+    for c in pieces(0):
+        c.wait_send()
+    for t in range(tiles):
+        for c in pieces(1, t):
             c.wait_send()
     tok.drain()
     wts.drain()
+    for store in stores:
+        store.wait()
 
 
 def angle_tables(rows, nsp):
@@ -553,34 +701,35 @@
     dma, V = pltpu.SemaphoreType.DMA, pltpu.VMEM
     vm, smem = pl.BlockSpec(memory_space=pltpu.VMEM), pl.BlockSpec(memory_space=pltpu.SMEM)
     hbm = pl.BlockSpec(memory_space=pl.ANY)
-    gather_sems = [dma((3, 2)), dma((4, 2)), dma((2,)), dma((4, 2)), dma((4, 2))]
+    gather_sems = [dma((3, 2)), dma((4, 2)), dma((3,)), dma((4, 2)), dma((4, 2))]
     message = rows + rows // 4 + rows
     return pl.pallas_call(
         functools.partial(layer_kernel, rows, nsp // NX, NX, ntp // 2),
         out_shape=jax.ShapeDtypeStruct((mine, D), bf16),
-        in_specs=[vm, vm, vm, vm, smem, smem] + [hbm] * 13,
-        out_specs=vm,
+        in_specs=[vm, vm, vm, vm, smem, smem] + [hbm] * 14,
+        out_specs=hbm,
         scratch_shapes=[
             V((4, 2, 2, half_rows, 256), bf16), V((4, 2, 2, 128, D), bf16),
             V((D, 768), bf16), V((D, 512), bf16), V((D, 384), bf16),
             V((256, D), bf16),
             V((192, 768), bf16), V((512, 128), bf16), V((512, 128), bf16),
-            V((32, 128), f32), V((32, rows), f32), V((rows, 1664), f32), V((rows, 128), f32),
+            V((32, 128), f32), V((32, rows), f32), V((32, rows), f32), V((rows, 1664), f32), V((rows, 128), f32),
             V((message, 128), bf16), V((tiles, 2, 64, QT), bf16), V((rows, 128), bf16),
             V((rows, 128), bf16), V((rows, 128), bf16), V((4, 2, 2, mine, 128), bf16),
             V((4, message, 128), bf16), V((4, rows, 128), bf16), V((4, tiles, 2, 96, QT), bf16),
             V((rows + 2 * WINDOW, 128), bf16),
             V((4, tiles, 8, QT), f32), V((4, tiles, 8, QT), f32), V((4, tiles, 128, QT), f32),
         ]
-        + [V((rows, QT), f32)] * 8 + [V((8, QT), f32)] * 8 + [V((mine, D), f32)]
+        + [V((rows, QT), f32)] * 8 + [V((8, QT), f32)] * 8 + [V((128, QT), f32), V((mine, D), bf16)]
         + [
             V((4, tiles, 128, QT), bf16), V((4, tiles, 8, QT), f32),
             V((4, tiles, 128, QT), bf16), V((4, tiles, 8, QT), f32),
-            dma((13,)),
+            dma((14,)),
         ]
-        + gather_sems + gather_sems
+        + gather_sems
+        + [dma((3, 3)), dma((3, 3)), dma((2,)), dma((2,)), dma((1,)), dma((1,)), dma((4, 2)), dma((4, 2))]
         + [
-            dma((2, 8)), dma((2, 4, 2)),
+            dma((1 + tiles, 8)), dma((1 + tiles, 4, 2)), dma((D // CB,)),
             dma((2,)), dma((2,)), dma((3, tiles)), dma((3, tiles)), dma((tiles, 2)), dma((tiles, 2)),
             dma((2, 2)), dma((2, 2)), dma((2,)), dma((2,)),
             dma((4, tiles)), dma((4, tiles)), dma((4, tiles)), dma((4, tiles)),
@@ -593,6 +742,7 @@
         tokens, norm_gain.reshape(1, D), query_gain.reshape(6, 128), latent_gain.reshape(1, -1),
         sink_logit, jnp.asarray(slopes), window_query, window_key.T, window_value.T, down_query, down_latent,
         rotary_proj.T, up_query.T, up_key, up_value, window_out, latent_out, jnp.asarray(far), jnp.asarray(near),
+        jnp.asarray(near.reshape(32, ntp, tiles, mine // tiles).transpose(0, 2, 1, 3).reshape(32, rows)),
     )
 
 

time: 73.5 us -> 72.1 us (0.981)
  Pallas kernels: 71.5 us -> 70.2 us
    pallas_call x1, Pallas kernels: 71.5 us -> 70.2 us  [per_device(): pl.pallas_call(functools.partial(layer_kernel, rows, nsp // NX, NX, ntp /...]
where the time goes in v5:
time: 72.1 us; the launch traced here: 71.9 us
  Pallas kernels  70.2 us (97%)
  local copies, waits for them, and re-layouts  1.77 us (2%)
    pallas_call x1, Pallas kernels, per_device(): pl.pallas_call(functools.partial(layer_kernel, rows, nsp // NX, NX, ntp /...  70.2 us
    unnamed x1, local copies, waits for them, and re-layouts  1.77 us

profile of v5, /device:TPU:1, one launch (start us, length us, event | category | flops | bytes accessed | tf_op | source)
XLA Modules:
  0.0 71.9 jit_solution(2647190335657967496)
XLA Ops:
  0.0 70.2 %layer.1 = bf16[96,2048]{1,0:T(8,128)(2,1)} custom-call(bf16[768,256]{1,0:T(8,128)(2,1)} %tokens.1, f32[1,2048]{1,0:T(1,128)} %bitcast.11, f32[6,128]{1,0:T(8,128)} %bitcast.12, f32[1,512]{1,0:T(1,128)} %bitcast.13, f32[2]{0:T(128)} %sinks.1, f32[16]{0:T(128)} %constant.8.clone.slopes, bf16[2048,128]{1,0:T(8,128)(2,1)} %w_query.1, bf16[64,2048]{1,0:T(8,128)(2,1)} %bitcast.8, ...), custom_call_target="tpu_custom_call" | custom-call | tf_op jit(solution)/shard_map/layer/pallas_call | solution.py:706
  70.2 1.8 %copy.22 = bf16[96,2048]{1,0:T(8,128)(2,1)} copy(bf16[96,2048]{1,0:T(8,128)(2,1)} %layer.1) | data formatting | bytes 786432

commit v6 on v5

--- a/solution.py
+++ b/solution.py
@@ -547,7 +547,7 @@
     for c in q_fwd.values():
         c.wait_recv()
     def arrive(i):
-        @pl.when(i == 4 * tiles)
+        @pl.when(i == 3 * tiles)
         def _():
             for c in k_fwd:
                 c.wait_recv()
@@ -573,11 +573,11 @@
 
     def mixed_order(i):
         p = i // tiles
-        return p - p // 3 - p // 5, 3 - p // 3 + p // 4 - p // 5, i % tiles
+        return p - 2 * (p // 4), 3 - p // 4, i % tiles
 
     def give_back(i):
         for q in (3, 2):
-            @pl.when(i // tiles == 7 - q)
+            @pl.when(i // tiles == 9 - 2 * q)
             def _():
                 finish(q, i % tiles)
                 for c in back(q, i % tiles):

time: 72.1 us -> 70.2 us (0.974)
  Pallas kernels: 70.2 us -> 68.3 us
    pallas_call x1, Pallas kernels: 70.2 us -> 68.3 us  [per_device(): pl.pallas_call(functools.partial(layer_kernel, rows, nsp // NX, NX, ntp /...]
where the time goes in v6:
time: 70.2 us; the launch traced here: 70.1 us
  Pallas kernels  68.3 us (97%)
  local copies, waits for them, and re-layouts  1.77 us (3%)
    pallas_call x1, Pallas kernels, per_device(): pl.pallas_call(functools.partial(layer_kernel, rows, nsp // NX, NX, ntp /...  68.3 us
    unnamed x1, local copies, waits for them, and re-layouts  1.77 us

profile of v6, /device:TPU:1, one launch (start us, length us, event | category | flops | bytes accessed | tf_op | source)
XLA Modules:
  0.0 70.1 jit_solution(15735564508700430410)
XLA Ops:
  0.0 68.3 %layer.1 = bf16[96,2048]{1,0:T(8,128)(2,1)} custom-call(bf16[768,256]{1,0:T(8,128)(2,1)} %tokens.1, f32[1,2048]{1,0:T(1,128)} %bitcast.11, f32[6,128]{1,0:T(8,128)} %bitcast.12, f32[1,512]{1,0:T(1,128)} %bitcast.13, f32[2]{0:T(128)} %sinks.1, f32[16]{0:T(128)} %constant.8.clone.slopes, bf16[2048,128]{1,0:T(8,128)(2,1)} %w_query.1, bf16[64,2048]{1,0:T(8,128)(2,1)} %bitcast.8, ...), custom_call_target="tpu_custom_call" | custom-call | tf_op jit(solution)/shard_map/layer/pallas_call | solution.py:706
  68.3 1.8 %copy.22 = bf16[96,2048]{1,0:T(8,128)(2,1)} copy(bf16[96,2048]{1,0:T(8,128)(2,1)} %layer.1) | data formatting | bytes 786432
